TPU v7x, 128 devices: a whole 4x4x4 slice. The times are simulated.
128 devices in a mesh: fs: 16 (over z, x), tp: 8 (over y, core).
Axes of the slice: x: 4, y: 4, z: 4, core: 2. Of those that a mesh axis runs over, the one named last changes fastest.
Arguments:
- tokens: bfloat16 [16384, 2048], P('fs', 'tp'), may hold values from -6 to 6
- recurrence_norm_gain: float32 [2048], replicated, may hold values from 0.1 to 1.9
- output_gate_weight: bfloat16 [2048, 2816], P('fs', 'tp'), may hold values from -0.125 to 0.125
- recurrence_input_weight: bfloat16 [2048, 2816], P('fs', 'tp'), may hold values from -0.125 to 0.125
- convolution_taps: float32 [4, 2816], P(None, 'tp'), may hold values from -3 to 3
- recurrence_gate_weight: bfloat16 [8, 352, 352], P('tp'), may hold values from -0.3125 to 0.3125
- input_gate_weight: bfloat16 [8, 352, 352], P('tp'), may hold values from -0.3125 to 0.3125
- base_decay_logit: float32 [2816], P('tp'), may hold values from 4.5 to 9.5
- token_log_decay: float32 [16384], P('fs'), may hold values from -0.7 to 0, as said below
- recurrence_output_weight: bfloat16 [2816, 2048], P('tp', 'fs'), may hold values from -0.4375 to 0.4375
- feedforward_norm_gain: float32 [2048], replicated, may hold values from 0.1 to 1.9
- feedforward_gate_weight: bfloat16 [2048, 5632], P('fs', 'tp'), may hold values from -0.125 to 0.125
- feedforward_up_weight: bfloat16 [2048, 5632], P('fs', 'tp'), may hold values from -0.125 to 0.125
- feedforward_down_weight: bfloat16 [5632, 2048], P('tp', 'fs'), may hold values from -0.15625 to 0.15625
Outputs:
- layer_out: bfloat16 [16384, 2048], P('fs', 'tp')
Inputs may be any that keep to these rules, and one draw needn't show every extreme that they name: `token_log_decay`: each entry is zero or lies between -0.7 and -0.22.
All inputs are finite; a program needn't handle non-finite values.
Results may differ from a plain program's by a relative error of at most 0.022.
Values may be sent and summed in bfloat16 or wider, within the bound.
A program may use at most 128 MiB of HBM per device.

v0:
```python
import jax
import jax.numpy as jnp
from jax import lax
from jax.sharding import PartitionSpec as P

LEN = 128


EPSILON = 1e-06
GATE_EXPONENT = 8.0


def joined_along(blocks, dim):
    shape = list(blocks.shape[1:])
    shape[dim] *= blocks.shape[0]
    return jnp.moveaxis(blocks, 0, dim).reshape(shape)


def sent_to_all(value, axis):
    peers = lax.axis_size(axis)
    return lax.all_to_all(
        jnp.broadcast_to(value[None], (peers, *value.shape)), axis, 0, 0, tiled=True
    )


def gather_directly(value, axis, dim):
    return joined_along(sent_to_all(value, axis), dim)


def in_blocks(value, dim, peers):
    before, after = (value.shape[:dim], value.shape[dim + 1 :])
    return jnp.moveaxis(value.reshape(*before, peers, -1, *after), dim, 0)


def sent_and_summed(value, axis, dim):
    blocks = in_blocks(value, dim, lax.axis_size(axis))
    arrived = lax.all_to_all(blocks, axis, split_axis=0, concat_axis=0, tiled=True)
    return arrived.astype(jnp.float32).sum(axis=0)


def norm_rows(values, gain_vec):
    widened = values.astype(jnp.float32)
    scaled = widened * lax.rsqrt(jnp.mean(widened * widened, axis=-1, keepdims=True) + EPSILON)
    return (scaled * gain_vec).astype(jnp.bfloat16)


def causal_taps(feature_vector, convolution_taps, length):
    row_count, channels = feature_vector.shape
    tap_count = convolution_taps.shape[0]
    blocks = feature_vector.reshape(row_count // length, length, channels)
    target = lax.broadcasted_iota(jnp.int32, (tap_count, length, length), 1)
    source = lax.broadcasted_iota(jnp.int32, (tap_count, length, length), 2)
    offset = lax.broadcasted_iota(jnp.int32, (tap_count, length, length), 0)
    shifters = (source == target - (tap_count - 1) + offset).astype(jnp.bfloat16)
    shifted = jnp.einsum("kts,bsc->kbtc", shifters, blocks, preferred_element_type=jnp.float32)
    summed = convolution_taps[0] * shifted[0]
    for position in range(1, tap_count):
        summed = summed + convolution_taps[position] * shifted[position]
    return summed.reshape(row_count, channels).astype(jnp.bfloat16)


def combine_steps(earlier, latter):
    return (earlier[0] * latter[0], latter[0] * earlier[1] + latter[1])


def linear_scan(decays, driven, length):
    row_count, channels = decays.shape
    shaped = (
        decays.reshape(row_count // length, length, channels),
        driven.reshape(row_count // length, length, channels),
    )
    result = lax.associative_scan(combine_steps, shaped, axis=1)
    return result[1].reshape(row_count, channels)


def block_dense(weight):
    groups, block_width, _ = weight.shape
    identity = jnp.eye(groups, dtype=jnp.bfloat16)[:, None, :, None]
    return (weight[:, :, None, :] * identity).reshape(groups * block_width, groups * block_width)


def stack_pieces(normed, shard_rows):
    row_count, width = normed.shape
    return jnp.transpose(normed.reshape(row_count, width // shard_rows, shard_rows), (1, 0, 2))


def add_rows(stacked, fragment):
    shard_rows = stacked.shape[2]
    count = fragment.shape[0] // shard_rows
    shaped = fragment.reshape(count, shard_rows, fragment.shape[1])
    return jnp.einsum("krc,kcf->rf", stacked, shaped, preferred_element_type=jnp.float32)


def fold_single(stacked, weight):
    return add_rows(stacked, gather_directly(weight, "fs", 0))


def two_projections(normed, weight_one, weight_two):
    stacked = stack_pieces(normed, weight_one.shape[0])
    return (fold_single(stacked, weight_one), fold_single(stacked, weight_two))


def project_down(values, weight):
    return jnp.dot(values, gather_directly(weight, "fs", 1), preferred_element_type=jnp.float32)


def recurrence(
    gate_projected,
    feature_vector,
    convolution_taps,
    recurrence_gate_weight,
    input_gate_weight,
    base_decay_logit,
    token_log_decay,
):
    mixed_in = causal_taps(feature_vector, convolution_taps, LEN)
    recurrence_gate = jax.nn.sigmoid(
        jnp.dot(mixed_in, block_dense(recurrence_gate_weight), preferred_element_type=jnp.float32)
    )
    inject_gate = jax.nn.sigmoid(
        jnp.dot(mixed_in, block_dense(input_gate_weight), preferred_element_type=jnp.float32)
    )
    decay_log_value = (
        -GATE_EXPONENT * jax.nn.softplus(-base_decay_logit)[None, :] * recurrence_gate
        + token_log_decay[:, None]
    )
    decays = jnp.exp(decay_log_value)
    driven = jnp.sqrt(-jnp.expm1(2.0 * decay_log_value)) * (
        inject_gate * mixed_in.astype(jnp.float32)
    )
    states = linear_scan(decays, driven, LEN)
    return (states * jax.nn.gelu(gate_projected)).astype(jnp.bfloat16)


def shards(
    tokens,
    recurrence_norm_gain,
    output_gate_weight,
    recurrence_input_weight,
    convolution_taps,
    recurrence_gate_weight,
    input_gate_weight,
    base_decay_logit,
    token_log_decay,
    recurrence_output_weight,
    feedforward_norm_gain,
    feedforward_gate_weight,
    feedforward_up_weight,
    feedforward_down_weight,
):
    own_width = tokens.shape[1]
    full_rows = lax.all_gather(tokens, "tp", axis=1, tiled=True)
    normed = norm_rows(full_rows, recurrence_norm_gain)
    gate_projected, feature_vector = two_projections(
        normed, output_gate_weight, recurrence_input_weight
    )
    carried = recurrence(
        gate_projected,
        feature_vector.astype(jnp.bfloat16),
        convolution_taps,
        recurrence_gate_weight,
        input_gate_weight,
        base_decay_logit,
        token_log_decay,
    )
    mixer_term = project_down(carried, recurrence_output_weight)
    full_sum = lax.psum(mixer_term.astype(jnp.bfloat16), "tp").astype(jnp.float32)
    residual_full = (full_rows.astype(jnp.float32) + full_sum).astype(jnp.bfloat16)
    residual_own = lax.dynamic_slice_in_dim(
        residual_full, lax.axis_index("tp") * own_width, own_width, 1
    )
    normed_two = norm_rows(residual_full, feedforward_norm_gain)
    gate_hidden, up_hidden = two_projections(
        normed_two, feedforward_gate_weight, feedforward_up_weight
    )
    hidden = (jax.nn.silu(gate_hidden) * up_hidden).astype(jnp.bfloat16)
    down_term = project_down(hidden, feedforward_down_weight)
    own_down = sent_and_summed(down_term.astype(jnp.bfloat16), "tp", 1)
    return (residual_own.astype(jnp.float32) + own_down).astype(jnp.bfloat16)


def solution(mesh):
    in_specs = (
        P("fs", "tp"),
        P(),
        P("fs", "tp"),
        P("fs", "tp"),
        P(None, "tp"),
        P("tp", None, None),
        P("tp", None, None),
        P("tp"),
        P("fs"),
        P("tp", "fs"),
        P(),
        P("fs", "tp"),
        P("fs", "tp"),
        P("tp", "fs"),
    )
    out_specs = P("fs", "tp")
    return jax.shard_map(shards, mesh=mesh, in_specs=in_specs, out_specs=out_specs, check_vma=False)
```

profile of v0, /device:TPU:1, one launch (start us, length us, event | category | flops | bytes accessed | tf_op | source)
XLA Modules:
  0.0 595.5 jit_solution(4509451641183435359)
XLA Ops:
  9.5 8.5 %all-to-all-start = ((bf16[16,128,352]{1,2,0:T(8,128)(2,1)}), bf16[16,128,352]{1,2,0:T(8,128)(2,1)S(1)}, u32[]{:S(2)}, u32[]{:S(2)}) async-start(bf16[16,128,352]{1,2,0:T(8,128)(2,1)} %broadcast_in_dim.12), calls=%async_computation | async-start | bytes 2883584 | tf_op jit(solution)/shard_map/all_to_all | solution.py:21
  18.1 30.1 %all-gather.2.cloned.1.call-done = bf16[1024,2048]{1,0:T(8,128)(2,1)} async-done(((bf16[1024,256]{1,0:T(8,128)(2,1)}), bf16[1024,2048]{1,0:T(8,128)(2,1)}) %all-gather.2.cloned.1.call-update) | async-done | bytes 4194320 | tf_op jit(solution)/shard_map/all_gather | solution.py:152
  52.6 6.8 %all-to-all-start.1 = ((bf16[16,128,352]{1,2,0:T(8,128)(2,1)}), bf16[16,128,352]{1,2,0:T(8,128)(2,1)}, u32[]{:S(2)}, u32[]{:S(2)}) async-start(bf16[16,128,352]{1,2,0:T(8,128)(2,1)} %broadcast_in_dim.13), calls=%async_computation.1 | async-start | bytes 2883584 | tf_op jit(solution)/shard_map/all_to_all | solution.py:21
  68.6 13.3 %all-to-all-done.1 = bf16[16,128,352]{1,2,0:T(8,128)(2,1)} async-done(((bf16[16,128,352]{1,2,0:T(8,128)(2,1)}), bf16[16,128,352]{1,2,0:T(8,128)(2,1)}, u32[]{:S(2)}, u32[]{:S(2)}) %all-to-all-start.1) | async-done | bytes 1441824 | tf_op jit(solution)/shard_map/all_to_all | solution.py:21
  96.5 26.3 %slice.194 = f32[8,64,352]{1,0,2:T(8,128)} slice(f32[8,128,352]{1,0,2:T(8,128)S(1)} %bitcast.213), slice={[0:8:1], [0:127:2], [0:352:1]} | slice | bytes 1441792 | tf_op jit(solution)/shard_map/slice | solution.py:72
  122.8 28.5 %slice.195 = f32[8,64,352]{1,0,2:T(8,128)} slice(f32[8,128,352]{1,0,2:T(8,128)S(1)} %bitcast.214), slice={[0:8:1], [1:128:2], [0:352:1]} | slice | bytes 1441792 | tf_op jit(solution)/shard_map/slice | solution.py:72
  151.8 28.7 %slice.193 = f32[8,64,352]{1,0,2:T(8,128)} slice(f32[8,128,352]{1,0,2:T(8,128)S(1)} %bitcast.217), slice={[0:8:1], [1:128:2], [0:352:1]} | slice | bytes 1441792 | tf_op jit(solution)/shard_map/slice | solution.py:72
  180.5 26.3 %slice.197 = f32[8,64,352]{1,0,2:T(8,128)} slice(f32[8,128,352]{1,0,2:T(8,128)S(1)} %bitcast.218), slice={[0:8:1], [0:127:2], [0:352:1]} | slice | bytes 1441792 | tf_op jit(solution)/shard_map/slice | solution.py:72
  223.0 6.7 %all-to-all-start.3 = ((bf16[16,128,704]{1,2,0:T(8,128)(2,1)}), bf16[16,128,704]{1,2,0:T(8,128)(2,1)}, u32[]{:S(2)}, u32[]{:S(2)}) async-start(bf16[16,128,704]{1,2,0:T(8,128)(2,1)} %broadcast_in_dim.15), calls=%async_computation.3 | async-start | bytes 5767168 | tf_op jit(solution)/shard_map/all_to_all | solution.py:21
  246.7 5.7 pad.52
  253.6 5.5 pad.51
  259.2 9.5 %all-to-all-done.3 = bf16[16,128,704]{1,2,0:T(8,128)(2,1)} async-done(((bf16[16,128,704]{1,2,0:T(8,128)(2,1)}), bf16[16,128,704]{1,2,0:T(8,128)(2,1)}, u32[]{:S(2)}, u32[]{:S(2)}) %all-to-all-start.3) | async-done | bytes 2883616 | tf_op jit(solution)/shard_map/all_to_all | solution.py:21
  280.7 28.5 %slice.241 = f32[8,63,352]{1,0,2:T(8,128)} slice(f32[8,128,352]{1,0,2:T(8,128)S(1)} %bitcast.215), slice={[0:8:1], [2:128:2], [0:352:1]} | slice | bytes 1419264 | tf_op jit(solution)/shard_map/slice | solution.py:72
  309.1 28.1 %slice.192 = f32[8,63,352]{1,0,2:T(8,128)} slice(f32[8,128,352]{1,0,2:T(8,128)S(1)} %bitcast.219), slice={[0:8:1], [2:128:2], [0:352:1]} | slice | bytes 1419264 | tf_op jit(solution)/shard_map/slice | solution.py:72
  338.6 10.5 %pad.54 = f32[8,64,352]{2,0,1:T(8,128)} pad(f32[8,32,352]{2,0,1:T(8,128)S(1)} %copy-done.11, f32[]{:T(128)} %constant.14.clone.1), padding=0_0_0x1_0_1x0_0_0 | pad | bytes 1081348 | tf_op jit(solution)/shard_map/pad | solution.py:72
  351.2 29.8 %pad.56 = f32[8,128,352]{2,0,1:T(8,128)} pad(f32[8,64,352]{2,0,1:T(8,128)} %add.202, f32[]{:T(128)} %constant.14.clone.1), padding=0_0_0x1_0_1x0_0_0 | pad | bytes 2162692 | tf_op jit(solution)/shard_map/pad | solution.py:72
  388.9 20.3 %pad.55 = f32[8,128,352]{2,0,1:T(8,128)} pad(f32[8,64,352]{2,0,1:T(8,128)S(1)} %pad_maximum_fusion, f32[]{:T(128)} %constant.14.clone.1), padding=0_0_0x0_1_1x0_0_0 | pad | bytes 2162692 | tf_op jit(solution)/shard_map/pad | solution.py:72
  413.9 9.4 %convolution_convert_fusion.1 = bf16[1024,2048]{1,0:T(8,128)(2,1)} fusion(f32[44,8,8,128]{3,2,1,0:T(8,128)S(1)} %bitcast.227, bf16[16,128,352]{1,2,0:T(8,128)(2,1)} %all-to-all-done.1, bf16[1024,2048]{1,0:T(8,128)(2,1)} %all-gather.2.cloned.1.call-done, f32[2048]{0:T(1024)S(1)} %copy-done.27, f32[1024]{0:T(1024)S(1)} %add_rsqrt_fusion.1, ...), kind=kOutput, calls=%fused_computation.23 | convolution fusion | flops 2966880256 | bytes 12726272 | tf_op jit(solution)/shard_map/dot_general | solution.py:104
  426.4 6.8 %all-to-all-start.5 = ((bf16[16,704,128]{2,1,0:T(8,128)(2,1)}), bf16[16,704,128]{2,1,0:T(8,128)(2,1)S(1)}, u32[]{:S(2)}, u32[]{:S(2)}) async-start(bf16[16,704,128]{2,1,0:T(8,128)(2,1)} %broadcast_in_dim.17), calls=%async_computation.5 | async-start | bytes 5767168 | tf_op jit(solution)/shard_map/all_to_all | solution.py:21
  433.2 64.5 %all-reduce.16.cloned.1.call-done = bf16[1024,2048]{1,0:T(8,128)(2,1)} async-done(((bf16[1024,2048]{1,0:T(8,128)(2,1)}), bf16[1024,2048]{1,0:T(8,128)(2,1)}) %all-reduce.16.cloned.1.call-update) | async-done | bytes 4194320 | tf_op jit(solution)/shard_map/psum | solution.py:167
  505.1 6.7 %fusion.10 = f32[1024,704,1]{0,1,2:T(8,128)} fusion(bf16[16,128,704]{1,2,0:T(8,128)(2,1)} %all-to-all-done.3, bf16[1024,2048]{1,0:T(8,128)(2,1)S(1)} %get-tuple-element.10, f32[2048]{0:T(1024)S(1)} %copy-done.28, f32[1024]{0:T(1024)S(1)} %add_rsqrt_fusion), kind=kOutput, calls=%fused_computation.18 | convolution fusion | flops 2961178624 | bytes 9973760 | tf_op jit(solution)/shard_map/krc,kcf->rf/dot_general | solution.py:91
  511.8 11.6 %convolution_convert_fusion = bf16[1024,2048]{1,0:T(8,128)(2,1)} fusion(f32[1024,704,1]{0,1,2:T(8,128)} %fusion.10, bf16[16,128,704]{1,2,0:T(8,128)(2,1)} %all-to-all-done.4, bf16[16,704,128]{2,1,0:T(8,128)(2,1)S(1)} %all-to-all-done.5, bf16[1024,2048]{1,0:T(8,128)(2,1)} %copy-done.6, f32[2048]{0:T(1024)S(1)} %copy-done.28, f32[1024]{0:T(1024)S(1)} %add_rsqrt_fusion), kind=kOutput, calls=%fused_computation.22 | convolution fusion | flops 5920391168 | bytes 17051648 | tf_op jit(solution)/shard_map/dot_general | solution.py:104
  527.9 6.8 %all-to-all-start.6 = ((bf16[8,1024,256]{2,1,0:T(8,128)(2,1)}), bf16[8,1024,256]{2,1,0:T(8,128)(2,1)}, u32[]{:S(2)}, u32[]{:S(2)}) async-start(bf16[8,1024,256]{2,1,0:T(8,128)(2,1)} %bitcast.220), calls=%async_computation.6 | async-start | bytes 8388608 | tf_op jit(solution)/shard_map/all_to_all | solution.py:37
  534.7 48.8 %all-to-all-done.6 = bf16[8,1024,256]{2,1,0:T(8,128)(2,1)} async-done(((bf16[8,1024,256]{2,1,0:T(8,128)(2,1)}), bf16[8,1024,256]{2,1,0:T(8,128)(2,1)}, u32[]{:S(2)}, u32[]{:S(2)}) %all-to-all-start.6) | async-done | bytes 4194336 | tf_op jit(solution)/shard_map/all_to_all | solution.py:37
  (145 shorter events, 113.7 us)
Async XLA Ops:
  6.5 81.4 %copy-start = (bf16[1,352,352]{2,1,0:T(8,128)(2,1)S(1)}, bf16[1,352,352]{2,1,0:T(8,128)(2,1)}, u32[]{:S(2)}) copy-start(bf16[1,352,352]{2,1,0:T(8,128)(2,1)} %param.19) | copy-start | bytes 743428
  6.5 41.6 %all-gather.2.cloned.1.call-start = ((), (), s32[]{:S(2)}) async-start(), calls=%async_computation.7 | async-start | bytes 4718592 | tf_op jit(solution)/shard_map/all_gather | solution.py:152
  9.5 8.6 %copy-start.23 = (f32[4,352]{1,0:T(4,128)S(1)}, f32[4,352]{1,0:T(4,128)}, u32[]{:S(2)}) copy-start(f32[4,352]{1,0:T(4,128)} %param.18) | copy-start | bytes 16900
  9.5 8.6 %copy-start.24 = (f32[352]{0:T(512)S(1)}, f32[352]{0:T(512)}, u32[]{:S(2)}) copy-start(f32[352]{0:T(512)} %param.21) | copy-start | bytes 4228
  9.5 41.8 %all-to-all-start = ((bf16[16,128,352]{1,2,0:T(8,128)(2,1)}), bf16[16,128,352]{1,2,0:T(8,128)(2,1)S(1)}, u32[]{:S(2)}, u32[]{:S(2)}) async-start(bf16[16,128,352]{1,2,0:T(8,128)(2,1)} %broadcast_in_dim.12), calls=%async_computation | async-start | bytes 2883584 | tf_op jit(solution)/shard_map/all_to_all | solution.py:21
  18.1 33.2 %copy-start.19 = (bf16[128,352]{0,1:T(8,128)(2,1)S(1)}, bf16[128,352]{0,1:T(8,128)(2,1)}, u32[]{:S(2)}) copy-start(bf16[128,352]{0,1:T(8,128)(2,1)} %param.16) | copy-start | bytes 270340
  52.6 6.9 %copy-start.26 = (f32[2048]{0:T(1024)S(1)}, f32[2048]{0:T(1024)}, u32[]{:S(2)}) copy-start(f32[2048]{0:T(1024)} %param.15) | copy-start | bytes 24580
  52.6 29.3 %all-to-all-start.1 = ((bf16[16,128,352]{1,2,0:T(8,128)(2,1)}), bf16[16,128,352]{1,2,0:T(8,128)(2,1)}, u32[]{:S(2)}, u32[]{:S(2)}) async-start(bf16[16,128,352]{1,2,0:T(8,128)(2,1)} %broadcast_in_dim.13), calls=%async_computation.1 | async-start | bytes 2883584 | tf_op jit(solution)/shard_map/all_to_all | solution.py:21
  67.4 14.5 %copy-start.20 = (bf16[352,128]{1,0:T(8,128)(2,1)S(1)}, bf16[352,128]{1,0:T(8,128)(2,1)}, u32[]{:S(2)}) copy-start(bf16[352,128]{1,0:T(8,128)(2,1)} %param.23) | copy-start | bytes 270340
  83.2 4.7 copy-start.14
  83.3 4.7 copy-start.29
  83.3 137.6 %all-to-all-start.2 = ((bf16[16,352,128]{2,1,0:T(8,128)(2,1)}), bf16[16,352,128]{2,1,0:T(8,128)(2,1)}, u32[]{:S(2)}, u32[]{:S(2)}) async-start(bf16[16,352,128]{2,1,0:T(8,128)(2,1)} %broadcast_in_dim.14), calls=%async_computation.2 | async-start | bytes 2883584 | tf_op jit(solution)/shard_map/all_to_all | solution.py:21
  88.8 5.0 copy-start.12
  122.8 28.5 %copy-start.13 = (f32[1024,352]{0,1:T(8,128)S(1)}, f32[1024,352]{0,1:T(8,128)}, u32[]{:S(2)}) copy-start(f32[1024,352]{0,1:T(8,128)} %copy-done.12) | copy-start | bytes 4325380
  223.0 45.6 %all-to-all-start.3 = ((bf16[16,128,704]{1,2,0:T(8,128)(2,1)}), bf16[16,128,704]{1,2,0:T(8,128)(2,1)}, u32[]{:S(2)}, u32[]{:S(2)}) async-start(bf16[16,128,704]{1,2,0:T(8,128)(2,1)} %broadcast_in_dim.15), calls=%async_computation.3 | async-start | bytes 5767168 | tf_op jit(solution)/shard_map/all_to_all | solution.py:21
  235.3 7.0 %copy-start.22 = (f32[8,1,352]{2,0,1:T(8,128)S(1)}, f32[8,1,352]{2,0,1:T(8,128)}, u32[]{:S(2)}) copy-start(f32[8,1,352]{2,0,1:T(8,128)} %slice.249) | copy-start | bytes 33796
  242.4 11.2 %copy-start.21 = (f32[8,1,352]{2,0,1:T(8,128)S(1)}, f32[8,1,352]{2,0,1:T(8,128)}, u32[]{:S(2)}) copy-start(f32[8,1,352]{2,0,1:T(8,128)} %slice.248) | copy-start | bytes 33796
  271.7 151.7 %all-to-all-start.4 = ((bf16[16,128,704]{1,2,0:T(8,128)(2,1)}), bf16[16,128,704]{1,2,0:T(8,128)(2,1)}, u32[]{:S(2)}, u32[]{:S(2)}) async-start(bf16[16,128,704]{1,2,0:T(8,128)(2,1)} %broadcast_in_dim.16), calls=%async_computation.4 | async-start | bytes 5767168 | tf_op jit(solution)/shard_map/all_to_all | solution.py:21
  277.0 220.7 %all-reduce.16.cloned.1.call-start = ((), (), s32[]{:S(2)}) async-start(), calls=%async_computation.8 | async-start | bytes 8388608 | tf_op jit(solution)/shard_map/psum | solution.py:167
  388.9 20.3 %copy-start.2 = (f32[8,128,352]{2,0,1:T(8,128)S(1)}, f32[8,128,352]{2,0,1:T(8,128)}, u32[]{:S(2)}) copy-start(f32[8,128,352]{2,0,1:T(8,128)} %pad.56) | copy-start | bytes 4325380
  426.4 85.4 %all-to-all-start.5 = ((bf16[16,704,128]{2,1,0:T(8,128)(2,1)}), bf16[16,704,128]{2,1,0:T(8,128)(2,1)S(1)}, u32[]{:S(2)}, u32[]{:S(2)}) async-start(bf16[16,704,128]{2,1,0:T(8,128)(2,1)} %broadcast_in_dim.17), calls=%async_computation.5 | async-start | bytes 5767168 | tf_op jit(solution)/shard_map/all_to_all | solution.py:21
  433.2 71.9 %copy-start.28 = (f32[2048]{0:T(1024)S(1)}, f32[2048]{0:T(1024)}, u32[]{:S(2)}) copy-start(f32[2048]{0:T(1024)} %param.24) | copy-start | bytes 24580
  527.9 55.6 %all-to-all-start.6 = ((bf16[8,1024,256]{2,1,0:T(8,128)(2,1)}), bf16[8,1024,256]{2,1,0:T(8,128)(2,1)}, u32[]{:S(2)}, u32[]{:S(2)}) async-start(bf16[8,1024,256]{2,1,0:T(8,128)(2,1)} %bitcast.220), calls=%async_computation.6 | async-start | bytes 8388608 | tf_op jit(solution)/shard_map/all_to_all | solution.py:37
  583.5 4.9 copy-start.1
  (15 other events, 25.6 us)
Sparse Core Ops, SparseCore 0:
  9.0 39.1 all-gather.1
  423.5 74.1 all-reduce.15
where the time goes:
time: 605 us; the launch traced here: 595 us
  local copies, waits for them, and re-layouts  295 us (49%)
  waiting for transfers between devices  167 us (28%)
  starting transfers between devices  45.8 us (8%)
  other arithmetic  38.3 us (6%)
  matrix products  35.6 us (6%)
  between operations  14.1 us (2%)
    slice x10, local copies, waits for them, and re-layouts, linear_scan(): result = lax.associative_scan(combine_steps, shaped, axis=1)  169 us
    pad x12, local copies, waits for them, and re-layouts, linear_scan(): result = lax.associative_scan(combine_steps, shaped, axis=1)  79.2 us
    psum x1, waiting for transfers between devices, shards(): lax.psum(mixer_term.astype(jnp.bfloat16), 'tp').astype(jnp.float32)  64.5 us
    all_to_all x1, waiting for transfers between devices, sent_and_summed(): lax.all_to_all(blocks, axis, split_axis=0, concat_axis=0, tiled=True)  48.8 us
    all_to_all x6, starting transfers between devices, sent_to_all(): lax.all_to_all(jnp.broadcast_to(value[None], (peers, *value.shape)), axis...  38.9 us
    all_gather x1, waiting for transfers between devices, shards(): full_rows = lax.all_gather(tokens, 'tp', axis=1, tiled=True)  30.1 us
    unnamed x71, local copies, waits for them, and re-layouts  23.6 us
    all_to_all x6, waiting for transfers between devices, sent_to_all(): lax.all_to_all(jnp.broadcast_to(value[None], (peers, *value.shape)), axis...  22.8 us
  transfers between devices with their start and end apart: 9, of which 5 were waited for; matrix products, arithmetic and copies ran while one was open for 56% of the time, Pallas kernels for 0%

commit v1 on v0

v1 whole, which is shorter than its diff:
```python
import functools

import jax
import jax.numpy as jnp
from jax import lax
from jax.experimental import pallas as pl
from jax.experimental.pallas import tpu as pltpu
from jax.sharding import PartitionSpec as P

MESH = pl.DeviceIdType.MESH
F32 = jnp.float32
BF16 = jnp.bfloat16

LEN = 128
EPSILON = 1e-06
GATE_EXPONENT = 8.0

SIDE = 4
CHUNKS = 4
ROWS = 1024
CH = ROWS // CHUNKS
HALF = CH // 2
SEQS = 8
RP = 384
FFL = 704
GU = 640
CB = 256


def row_ranges(kind):
    if kind == "row":
        return {0: ((0, 32), (32, 32)), 1: ((64, 32), (96, 32))}
    if kind == "wo":
        return {0: ((0, 96), (96, 80)), 1: ((176, 96), (272, 80))}
    return {0: ((0, 176), (176, 176)), 1: ((352, 176), (528, 176))}


class Gather:
    def __init__(self, buf, kind, send, recv, pos, dev):
        self.buf, self.kind, self.send, self.recv, self.pos, self.dev = buf, kind, send, recv, pos, dev
        self.rows = row_ranges(kind)

    def span(self, part, half):
        lo, hi = self.rows[part]
        if half == 0:
            return pl.ds(lo[0], lo[1])
        if half == 1:
            return pl.ds(hi[0], hi[1])
        return pl.ds(lo[0], lo[1] + hi[1])

    def block(self, part, i1, i2, half=None):
        z, x = (i2, i1) if part == 0 else (i1, i2)
        rows = self.span(part, half)
        if self.kind == "row":
            return self.buf.at[z, x, rows, :]
        cols = pl.ds(pl.multiple_of(lax.rem(x, 2) * 128, 128), 128)
        return self.buf.at[z, x // 2, rows, cols]

    def line(self, part, i2, half=None):
        rows = self.span(part, None)
        if part == 0:
            if self.kind == "row":
                xs = pl.ds(0, 4) if half is None else pl.ds(2 * half, 2)
            else:
                xs = pl.ds(0, 2) if half is None else pl.ds(half, 1)
            return self.buf.at[i2, xs, rows, :]
        zs = pl.ds(0, 4) if half is None else pl.ds(2 * half, 2)
        if self.kind == "row":
            return self.buf.at[zs, i2, rows, :]
        cols = pl.ds(pl.multiple_of(lax.rem(i2, 2) * 128, 128), 128)
        return self.buf.at[zs, i2 // 2, rows, cols]

    def copy(self, view, part, k, to):
        return pltpu.make_async_remote_copy(
            src_ref=view,
            dst_ref=view,
            send_sem=self.send.at[part, k],
            recv_sem=self.recv.at[part, k],
            device_id=to,
            device_id_type=MESH,
        )

    def around(self, part):
        a1, a2 = ("x", "z") if part == 0 else ("z", "x")
        return a1, a2, self.pos[a1], self.pos[a2]

    def moves(self, part):
        a1, a2, (m1, i1, p1), (m2, i2, p2) = self.around(part)
        far1, far2 = lax.rem(i1 + 2, SIDE), lax.rem(i2 + 2, SIDE)
        return [
            self.block(part, m1, i2),
            self.block(part, p1, i2),
            self.block(part, far1, i2, 0),
            self.block(part, far1, i2, 1),
            self.line(part, m2),
            self.line(part, p2),
            self.line(part, far2, 0),
            self.line(part, far2, 1),
        ]

    def arrived(self, part, k):
        self.copy(self.moves(part)[k], part, k, self.dev["x"][0]).wait_recv()

    def stage0(self):
        for part in (0, 1):
            a1, a2, (m1, i1, p1), (m2, i2, p2) = self.around(part)
            view = self.block(part, i1, i2)
            self.copy(view, part, 0, self.dev[a1][1]).start()
            self.copy(view, part, 1, self.dev[a1][0]).start()

    def stage1(self):
        for part in (0, 1):
            a1, a2, (m1, i1, p1), (m2, i2, p2) = self.around(part)
            self.arrived(part, 0)
            self.copy(self.block(part, m1, i2, 0), part, 2, self.dev[a1][1]).start()
            self.arrived(part, 1)
            self.copy(self.block(part, p1, i2, 1), part, 3, self.dev[a1][0]).start()

    def stage2(self):
        for part in (0, 1):
            a1, a2, (m1, i1, p1), (m2, i2, p2) = self.around(part)
            self.arrived(part, 2)
            self.arrived(part, 3)
            view = self.line(part, i2)
            self.copy(view, part, 4, self.dev[a2][1]).start()
            self.copy(view, part, 5, self.dev[a2][0]).start()

    def stage3(self):
        for part in (0, 1):
            a1, a2, (m1, i1, p1), (m2, i2, p2) = self.around(part)
            self.arrived(part, 4)
            self.copy(self.line(part, m2, 0), part, 6, self.dev[a2][1]).start()
            self.arrived(part, 5)
            self.copy(self.line(part, p2, 1), part, 7, self.dev[a2][0]).start()

    def stage4(self):
        for part in (0, 1):
            self.arrived(part, 6)
            self.arrived(part, 7)

    def drain(self):
        for part in (0, 1):
            for k, view in enumerate(self.moves(part)):
                self.copy(view, part, k, self.dev["x"][0]).wait_send()


class Spread:
    def __init__(self, buf, send, recv, y, core, dev):
        self.buf, self.send, self.recv, self.dev = buf, send, recv, dev
        (ym, yy, yp), far = y, lax.rem(y[1] + 2, SIDE)
        other = 1 - core
        self.own, self.minus, self.plus, self.far = (2 * v + core for v in (yy, ym, yp, far))
        self.others = [2 * v + other for v in (yy, ym, yp, far)]

    def view(self, block, c, half=None):
        if half is None:
            return self.buf.at[block, pl.ds(pl.multiple_of(c * CH, CH), CH), :]
        return self.buf.at[block, pl.ds(pl.multiple_of(c * CH + half * HALF, HALF), HALF), :]

    def copy(self, view, k, c, to):
        return pltpu.make_async_remote_copy(
            src_ref=view,
            dst_ref=view,
            send_sem=self.send.at[k, c],
            recv_sem=self.recv.at[k, c],
            device_id=to,
            device_id_type=MESH,
        )

    def landing(self, k, c):
        return [
            (self.minus, None),
            (self.plus, None),
            (self.others[0], None),
            (self.far, 0),
            (self.far, 1),
            (self.others[1], None),
            (self.others[2], None),
            (self.others[3], None),
        ][k]

    def arrived(self, k, c):
        block, half = self.landing(k, c)
        self.copy(self.view(block, c, half), k, c, self.dev["core"]).wait_recv()

    def stage0(self, c):
        view = self.view(self.own, c)
        self.copy(view, 0, c, self.dev["y"][1]).start()
        self.copy(view, 1, c, self.dev["y"][0]).start()
        self.copy(view, 2, c, self.dev["core"]).start()

    def stage1(self, c):
        self.arrived(0, c)
        self.copy(self.view(self.minus, c, 0), 3, c, self.dev["y"][1]).start()
        self.copy(self.view(self.minus, c), 5, c, self.dev["core"]).start()
        self.arrived(1, c)
        self.copy(self.view(self.plus, c, 1), 4, c, self.dev["y"][0]).start()
        self.copy(self.view(self.plus, c), 6, c, self.dev["core"]).start()

    def stage2(self, c):
        self.arrived(3, c)
        self.arrived(4, c)
        self.copy(self.view(self.far, c), 7, c, self.dev["core"]).start()

    def stage3(self, c):
        for k in (2, 5, 6, 7):
            self.arrived(k, c)

    def drain(self, c):
        for k in range(8):
            block, half = self.landing(k, c)
            self.copy(self.view(block, c, half), k, c, self.dev["core"]).wait_send()


class Sum:
    def __init__(self, give, keep, took, total, halves, finals, send, recv, y, core, dev):
        self.give, self.keep, self.took, self.total = give, keep, took, total
        self.halves, self.finals, self.send, self.recv, self.dev = halves, finals, send, recv, dev
        self.minus, self.own, self.plus = y
        self.far = lax.rem(y[1] + 2, SIDE)

    def rows(self, c):
        return pl.ds(pl.multiple_of(c * CH, CH), CH)

    def half(self, c, h):
        return pl.ds(pl.multiple_of(c * CH + h * HALF, HALF), HALF)

    def parts(self, k, c):
        if k == 0:
            return self.give.at[:, self.rows(c), :], self.took.at[:, self.rows(c), :], self.dev["core"]
        if k <= 2:
            return self.total.at[self.far, self.half(c, k - 1), :], self.halves.at[k - 1, c], self.dev["y"][2 - k]
        to = self.plus if k == 3 else self.minus
        return self.total.at[to, self.rows(c), :], self.finals.at[k - 3, self.rows(c), :], self.dev["y"][4 - k]

    def copy(self, k, c):
        src, dst, to = self.parts(k, c)
        return pltpu.make_async_remote_copy(
            src_ref=src,
            dst_ref=dst,
            send_sem=self.send.at[k, c],
            recv_sem=self.recv.at[k, c],
            device_id=to,
            device_id_type=MESH,
        )

    def stage0(self, c):
        self.copy(0, c).start()

    def stage1(self, c):
        self.copy(0, c).wait_recv()
        rows = self.rows(c)
        for target in (self.far, self.plus, self.minus, self.own):
            self.total[target, rows, :] = (
                self.keep[target, rows, :].astype(F32) + self.took[target, rows, :].astype(F32)
            ).astype(BF16)
        self.copy(1, c).start()
        self.copy(2, c).start()

    def stage2(self, c):
        for h, target in ((0, self.plus), (1, self.minus)):
            self.copy(1 + h, c).wait_recv()
            rows = self.half(c, h)
            self.total[target, rows, :] = (
                self.total[target, rows, :].astype(F32) + self.halves[h, c].astype(F32)
            ).astype(BF16)
        self.copy(3, c).start()
        self.copy(4, c).start()

    def stage3(self, c):
        self.copy(3, c).wait_recv()
        self.copy(4, c).wait_recv()
        rows = self.rows(c)
        return (
            self.total[self.own, rows, :].astype(F32)
            + self.finals[0, rows, :].astype(F32)
            + self.finals[1, rows, :].astype(F32)
        )

    def drain(self, c):
        for k in range(5):
            self.copy(k, c).wait_send()


def norm_chunk(full, gain, out, c):
    step = 16

    def body(i, carry):
        rows = pl.ds(pl.multiple_of(c * CH + i * step, step), step)
        here = pl.ds(pl.multiple_of(i * step, step), step)
        total = jnp.zeros((step, CB), F32)
        for b in range(8):
            v = full[b, rows, :].astype(F32)
            total = total + v * v
        scale = lax.rsqrt(jnp.sum(total, axis=1, keepdims=True) * (1.0 / 2048.0) + EPSILON)
        for b in range(8):
            v = full[b, rows, :].astype(F32)
            out[here, b * CB : (b + 1) * CB] = ((v * scale) * gain[b : b + 1, :]).astype(BF16)
        return carry

    lax.fori_loop(0, CH // step, body, 0, unroll=2)


def kernel(
    tok_hbm, wgi_hbm, wo_hbm, wff_hbm, wd_hbm, gm, small, ld, gain1, gain2,
    out,
    full1, full2, wgi, wo, wff, wd,
    give1, keep1, took1, total1, halves1, finals1,
    give2, keep2, took2, total2, halves2, finals2,
    feat, proj, mixed, gl, carried, nrm, ffo, hid, state,
    local_sem, w_send, w_recv, a_send, a_recv, s_send, s_recv,
):
    fs, tp = lax.axis_index("fs"), lax.axis_index("tp")
    iz, ix = fs // SIDE, lax.rem(fs, SIDE)
    iy, core = tp // 2, lax.rem(tp, 2)

    def ring(i):
        return lax.rem(i + SIDE - 1, SIDE), i, lax.rem(i + 1, SIDE)

    pos = {"x": ring(ix), "z": ring(iz)}
    y = ring(iy)
    dev = {
        "x": tuple({"fs": iz * SIDE + pos["x"][k]} for k in (0, 2)),
        "z": tuple({"fs": pos["z"][k] * SIDE + ix} for k in (0, 2)),
        "y": tuple({"tp": 2 * y[k] + core} for k in (0, 2)),
        "core": {"tp": 2 * iy + 1 - core},
    }

    barrier = pltpu.get_barrier_semaphore()
    for to in (*dev["x"], *dev["z"], *dev["y"], dev["core"]):
        pl.semaphore_signal(barrier, inc=1, device_id=to, device_id_type=MESH)

    cols = pl.ds(pl.multiple_of(lax.rem(ix, 2) * 128, 128), 128)
    own = [
        pltpu.make_async_copy(wgi_hbm, wgi.at[iz, ix], local_sem.at[0]),
        pltpu.make_async_copy(tok_hbm, full1.at[tp], local_sem.at[1]),
        pltpu.make_async_copy(wo_hbm, wo.at[iz, ix // 2, pl.ds(0, 352), cols], local_sem.at[2]),
        pltpu.make_async_copy(wff_hbm, wff.at[iz, ix], local_sem.at[3]),
        pltpu.make_async_copy(wd_hbm, wd.at[iz, ix // 2, :, cols], local_sem.at[4]),
    ]
    for copy in own:
        copy.start()
    wo[:, :, 352:RP, :] = jnp.zeros((SIDE, 2, RP - 352, CB), BF16)
    feat[0:24, :] = jnp.zeros((24, RP), F32)
    state[...] = jnp.zeros_like(state)

    gathers = [
        Gather(buf, kind, w_send.at[m], w_recv.at[m], pos, dev)
        for m, (buf, kind) in enumerate(((wgi, "row"), (wo, "wo"), (wff, "row"), (wd, "wd")))
    ]
    g_wgi, g_wo, g_wff, g_wd = gathers
    spread1 = Spread(full1, a_send.at[0], a_recv.at[0], y, core, dev)
    spread2 = Spread(full2, a_send.at[1], a_recv.at[1], y, core, dev)
    sum1 = Sum(give1, keep1, took1, total1, halves1, finals1, s_send.at[0], s_recv.at[0], y, core, dev)
    sum2 = Sum(give2, keep2, took2, total2, halves2, finals2, s_send.at[1], s_recv.at[1], y, core, dev)

    pl.semaphore_wait(barrier, 7)

    def each_chunk(stage):
        def body(c, carry):
            stage(c)
            return carry

        lax.fori_loop(0, CHUNKS, body, 0)

    own[0].wait()
    g_wgi.stage0()
    own[1].wait()
    each_chunk(spread1.stage0)
    own[2].wait()
    g_wo.stage0()
    own[3].wait()
    g_wff.stage0()
    own[4].wait()
    g_wd.stage0()
    g_wgi.stage1()
    g_wo.stage1()
    each_chunk(spread1.stage1)
    g_wff.stage1()
    g_wgi.stage2()
    g_wo.stage2()
    g_wd.stage1()
    each_chunk(spread1.stage2)
    g_wff.stage2()
    g_wd.stage2()
    g_wgi.stage3()
    g_wo.stage3()
    each_chunk(spread1.stage3)
    g_wgi.stage4()

    def mix(c):
        norm_chunk(full1, gain1, nrm, c)
        base = pl.multiple_of(c * CH, CH)
        projected = jnp.dot(nrm[...], wgi[...].reshape(2048, 2 * RP), preferred_element_type=F32)
        proj[...] = projected[:, :RP]
        feat[pl.ds(base + 24, CH), :] = projected[:, RP:].astype(BF16).astype(F32)

        def taps(i, carry):
            r = pl.multiple_of(i * 32, 32)
            summed = small[0:1, :] * feat[pl.ds(base + r, 32), :]
            for k in range(1, 4):
                summed = summed + small[k : k + 1, :] * feat[pl.ds(base + r + 8 * k, 32), :]
            mixed[pl.ds(r, 32), :] = summed.astype(BF16)
            return carry

        lax.fori_loop(0, CH // 32, taps, 0, unroll=2)
        gl[...] = jnp.dot(mixed[...], gm[...], preferred_element_type=F32)

        def steps(i, h):
            r = pl.multiple_of(i * 32, 32)
            rows = pl.ds(r, 32)
            recur = jax.nn.sigmoid(gl[rows, :RP])
            inject = jax.nn.sigmoid(gl[rows, RP:])
            log_decay = small[4:5, :] * recur + ld[pl.ds(base + r, 32), :]
            decay = jnp.exp(log_decay)
            twice = 2.0 * log_decay
            near = -twice * (1.0 + twice * (0.5 + twice * (1.0 / 6.0 + twice * (1.0 / 24.0 + twice * (1.0 / 120.0)))))
            rest = jnp.where(twice > -0.1, near, 1.0 - decay * decay)
            driven = jnp.sqrt(rest) * (inject * mixed[rows, :].astype(F32))
            states = []
            for s in range(4):
                h = decay[8 * s : 8 * s + 8] * h + driven[8 * s : 8 * s + 8]
                states.append(h)
            carried[rows, :] = (jnp.concatenate(states, axis=0) * jax.nn.gelu(proj[rows, :])).astype(BF16)
            return h

        state[...] = lax.fori_loop(0, CH // 32, steps, state[...])

        @pl.when(c == 0)
        def _():
            g_wo.stage4()

        rows = pl.ds(base, CH)
        for target in range(SIDE):
            for side, ref in ((core, keep1), (1 - core, give1)):
                ref[target, rows, :] = jnp.dot(
                    carried[...], wo[target, side], preferred_element_type=F32
                ).astype(BF16)
        sum1.stage0(c)

    def settle(c):
        rows = pl.ds(pl.multiple_of(c * CH, CH), CH)
        full2[tp, rows, :] = (full1[tp, rows, :].astype(F32) + sum1.stage3(c)).astype(BF16)
        spread2.stage0(c)

    def feed(c):
        spread2.stage3(c)
        norm_chunk(full2, gain2, nrm, c)
        ffo[...] = jnp.dot(nrm[...], wff[...].reshape(2048, 2 * FFL), preferred_element_type=F32)

        def act(i, carry):
            rows = pl.ds(pl.multiple_of(i * 16, 16), 16)
            hid[rows, :GU] = (jax.nn.silu(ffo[rows, :GU]) * ffo[rows, GU : 2 * GU]).astype(BF16)
            tail = ffo[rows, 2 * GU :]
            hid[rows, GU:] = (jax.nn.silu(tail[:, :64]) * tail[:, 64:]).astype(BF16)
            return carry

        lax.fori_loop(0, CH // 16, act, 0, unroll=2)

        @pl.when(c == 0)
        def _():
            g_wd.stage4()

        rows = pl.ds(pl.multiple_of(c * CH, CH), CH)
        for target in range(SIDE):
            for side, ref in ((core, keep2), (1 - core, give2)):
                ref[target, rows, :] = jnp.dot(
                    hid[...], wd[target, side], preferred_element_type=F32
                ).astype(BF16)
        sum2.stage0(c)

    def finish(c):
        rows = pl.ds(pl.multiple_of(c * CH, CH), CH)
        out[rows, :] = (full2[tp, rows, :].astype(F32) + sum2.stage3(c)).astype(BF16)

    stages = [
        (9, sum2.stage2),
        (8, sum2.stage1),
        (5, spread2.stage2),
        (4, spread2.stage1),
        (3, settle),
        (2, sum1.stage2),
        (1, sum1.stage1),
        (0, mix),
        (7, feed),
        (10, finish),
    ]

    def tick(i, carry):
        @pl.when(i == 4)
        def _():
            g_wff.stage3()

        @pl.when(i == 6)
        def _():
            g_wd.stage3()

        @pl.when(i == 7)
        def _():
            g_wff.stage4()

        for lag, stage in stages:
            pl.when((i >= lag) & (i < lag + CHUNKS))(functools.partial(stage, i - lag))
        return carry

    lax.fori_loop(0, CHUNKS + 10, tick, 0)

    for gather in gathers:
        gather.drain()

    def drained(c, carry):
        for group in (spread1, spread2, sum1, sum2):
            group.drain(c)
        return carry

    lax.fori_loop(0, CHUNKS, drained, 0)


def layer(tok, wgi, wo, wff, wd, gm, small, ld, gain1, gain2):
    anywhere = pl.BlockSpec(memory_space=pl.ANY)
    vmem = pl.BlockSpec(memory_space=pltpu.VMEM)
    sums = [
        pltpu.VMEM((SIDE, ROWS, CB), BF16),
        pltpu.VMEM((SIDE, ROWS, CB), BF16),
        pltpu.VMEM((SIDE, ROWS, CB), BF16),
        pltpu.VMEM((SIDE, ROWS, CB), BF16),
        pltpu.VMEM((2, CHUNKS, HALF, CB), BF16),
        pltpu.VMEM((2, ROWS, CB), BF16),
    ]
    return pl.pallas_call(
        kernel,
        out_shape=jax.ShapeDtypeStruct((ROWS, CB), BF16),
        in_specs=[anywhere] * 5 + [vmem] * 5,
        out_specs=vmem,
        scratch_shapes=[
            pltpu.VMEM((8, ROWS, CB), BF16),
            pltpu.VMEM((8, ROWS, CB), BF16),
            pltpu.VMEM((SIDE, SIDE, 128, 2 * RP), BF16),
            pltpu.VMEM((SIDE, 2, RP, CB), BF16),
            pltpu.VMEM((SIDE, SIDE, 128, 2 * FFL), BF16),
            pltpu.VMEM((SIDE, 2, FFL, CB), BF16),
            *sums,
            *sums,
            pltpu.VMEM((24 + ROWS, RP), F32),
            pltpu.VMEM((CH, RP), F32),
            pltpu.VMEM((CH, RP), BF16),
            pltpu.VMEM((CH, 2 * RP), F32),
            pltpu.VMEM((CH, RP), BF16),
            pltpu.VMEM((CH, 2048), BF16),
            pltpu.VMEM((CH, 2 * FFL), F32),
            pltpu.VMEM((CH, FFL), BF16),
            pltpu.VMEM((SEQS, RP), F32),
            pltpu.SemaphoreType.DMA((5,)),
            pltpu.SemaphoreType.DMA((4, 2, 8)),
            pltpu.SemaphoreType.DMA((4, 2, 8)),
            pltpu.SemaphoreType.DMA((2, 8, CHUNKS)),
            pltpu.SemaphoreType.DMA((2, 8, CHUNKS)),
            pltpu.SemaphoreType.DMA((2, 5, CHUNKS)),
            pltpu.SemaphoreType.DMA((2, 5, CHUNKS)),
        ],
        compiler_params=pltpu.CompilerParams(
            collective_id=0, has_side_effects=True, vmem_limit_bytes=66_000_000
        ),
    )(tok, wgi, wo, wff, wd, gm, small, ld, gain1, gain2)


def shards(
    tokens,
    recurrence_norm_gain,
    output_gate_weight,
    recurrence_input_weight,
    convolution_taps,
    recurrence_gate_weight,
    input_gate_weight,
    base_decay_logit,
    token_log_decay,
    recurrence_output_weight,
    feedforward_norm_gain,
    feedforward_gate_weight,
    feedforward_up_weight,
    feedforward_down_weight,
):
    tok = tokens.reshape(SEQS, LEN, CB).transpose(1, 0, 2).reshape(ROWS, CB)
    ld = token_log_decay.reshape(SEQS, LEN).T.reshape(ROWS, 1)
    pad = ((0, 0), (0, RP - 352))
    wgi = jnp.concatenate([jnp.pad(output_gate_weight, pad), jnp.pad(recurrence_input_weight, pad)], axis=1)
    square = ((0, RP - 352), (0, RP - 352))
    gm = jnp.concatenate(
        [jnp.pad(recurrence_gate_weight[0], square), jnp.pad(input_gate_weight[0], square)], axis=1
    )
    wff = jnp.concatenate(
        [
            feedforward_gate_weight[:, :GU],
            feedforward_up_weight[:, :GU],
            feedforward_gate_weight[:, GU:],
            feedforward_up_weight[:, GU:],
        ],
        axis=1,
    )
    rate = -GATE_EXPONENT * jax.nn.softplus(-base_decay_logit)
    small = jnp.pad(jnp.concatenate([convolution_taps, rate[None, :]], axis=0), ((0, 3), (0, RP - 352)))
    out = layer(
        tok,
        wgi,
        recurrence_output_weight,
        wff,
        feedforward_down_weight,
        gm,
        small,
        ld,
        recurrence_norm_gain.reshape(8, CB),
        feedforward_norm_gain.reshape(8, CB),
    )
    return out.reshape(LEN, SEQS, CB).transpose(1, 0, 2).reshape(ROWS, CB)


def solution(mesh):
    in_specs = (
        P("fs", "tp"),
        P(),
        P("fs", "tp"),
        P("fs", "tp"),
        P(None, "tp"),
        P("tp", None, None),
        P("tp", None, None),
        P("tp"),
        P("fs"),
        P("tp", "fs"),
        P(),
        P("fs", "tp"),
        P("fs", "tp"),
        P("tp", "fs"),
    )
    return jax.shard_map(shards, mesh=mesh, in_specs=in_specs, out_specs=P("fs", "tp"), check_vma=False)
```

time: 605 us -> 170 us (0.28); the launches traced: 595 us -> 170 us
  local copies, waits for them, and re-layouts: 295 us -> 12.4 us
  waiting for transfers between devices: 167 us -> 0 us
  Pallas kernels: 0 us -> 154 us
  starting transfers between devices: 45.8 us -> 0 us
  matrix products: 35.6 us -> 0 us
  other arithmetic: 38.3 us -> 3.6 us
  between operations: 14.1 us -> 0.06 us
    slice x15 -> x6, local copies, waits for them, and re-layouts: 172 us -> 1.55 us  [the longest x1 0.73 us: shards(): feedforward_up_weight[:, GU:]]
    pallas_call x0 -> x1, Pallas kernels: none -> 154 us  [layer(): pl.pallas_call(kernel, out_shape=jax.ShapeDtypeStruct((ROWS, CB), BF16),...]
    pad x12 -> x0, local copies, waits for them, and re-layouts: 79.2 us -> none  [linear_scan(): result = lax.associative_scan(combine_steps, shaped, axis=1)]
    all_to_all x7 -> x0, waiting for transfers between devices: 71.6 us -> none  [the longest x1 48.8 us: sent_and_summed(): lax.all_to_all(blocks, axis, split_axis=0, concat_axis=0, tiled=True)]
    psum x1 -> x0, waiting for transfers between devices: 64.5 us -> none  [shards(): lax.psum(mixer_term.astype(jnp.bfloat16), 'tp').astype(jnp.float32)]
    all_to_all x7 -> x0, starting transfers between devices: 45.7 us -> none  [the longest x6 38.9 us: sent_to_all(): lax.all_to_all(jnp.broadcast_to(value[None], (peers, *value.shape)), axis...]
    dot_general x7 -> x0, matrix products: 35.6 us -> none  [the longest x2 21 us: project_down(): jnp.dot(values, gather_directly(weight, 'fs', 1), preferred_element_type=...]
    all_gather x1 -> x0, waiting for transfers between devices: 30.1 us -> none  [shards(): full_rows = lax.all_gather(tokens, 'tp', axis=1, tiled=True)]
  transfers between devices with their start and end apart: 9 -> 0, of which waited for: 5 -> 0; matrix products, arithmetic and copies ran while one was open for 56% -> 0% of each run, Pallas kernels for 0% -> 0%
where the time goes in v1:
time: 170 us
  Pallas kernels  154 us (91%)
  local copies, waits for them, and re-layouts  12.4 us (7%)
  other arithmetic  3.6 us (2%)
    pallas_call x1, Pallas kernels, layer(): pl.pallas_call(kernel, out_shape=jax.ShapeDtypeStruct((ROWS, CB), BF16),...  154 us

profile of v1, /device:TPU:1, one launch (start us, length us, event | category | flops | bytes accessed | tf_op | source)
XLA Modules:
  0.0 169.9 jit_solution(2115744898694417623)
XLA Ops:
  0.0 0.7 fusion.6
  0.7 1.3 reshape.28.gain1
  2.0 1.3 reshape.29.gain2
  3.3 1.3 select_maximum_fusion.small
  4.6 0.7 slice.14
  5.3 0.1 copy.35
  5.4 0.7 slice.15
  6.2 0.1 copy.36
  6.3 0.0 slice-start
  6.3 0.8 copy.30
  7.1 1.0 copy.24
  8.1 1.0 copy.25
  9.1 0.0 slice-start.1
  9.1 0.7 fusion.5.wgi_hbm
  9.9 0.2 copy.33
  10.0 0.1 slice-done.1
  10.1 0.2 copy.34
  10.3 0.0 copy-start
  10.3 0.8 concatenate.13.wff_hbm
  11.1 1.0 reshape.32.ld
  12.1 1.1 copy.38
  13.2 0.9 fusion.2.gm
  14.1 153.9 %shard_map.136 = bf16[1024,256]{1,0:T(8,128)(2,1)} custom-call(bf16[1024,256]{1,0:T(8,128)(2,1)} %bitcast.16, bf16[128,768]{1,0:T(8,128)(2,1)} %fusion.5.wgi_hbm, bf16[352,128]{1,0:T(8,128)(2,1)} %wo_hbm.1, bf16[128,1408]{1,0:T(8,128)(2,1)} %concatenate.13.wff_hbm, bf16[704,128]{1,0:T(8,128)(2,1)} %wd_hbm.1, bf16[384,768]{1,0:T(8,128)(2,1)} %fusion.2.gm, ...), custom_call_target="tpu_custom_call" | custom-call | tf_op jit(solution)/shard_map/pallas_call | solution.py:530
  168.0 1.9 %copy.32 = bf16[8,128,256]{2,1,0:T(8,128)(2,1)} copy(bf16[8,128,256]{2,0,1:T(8,128)(2,1)} %bitcast.15) | data formatting | bytes 1048576 | tf_op jit(solution)/shard_map/transpose | solution.py:614
  (7 shorter events, 0.0 us)
Async XLA Ops:
  6.3 3.6 %slice-start = ((bf16[128,704]{0,1:T(8,128)(2,1)}), bf16[128,640]{0,1:T(8,128)(2,1)S(1)}, s32[]{:S(2)}) async-start(bf16[128,704]{0,1:T(8,128)(2,1)} %param.25), calls=%async_computation | async-start | bytes 327680 | tf_op jit(solution)/shard_map/slice | solution.py:593
  9.1 1.0 slice-start.1
  10.3 1.8 %copy-start = (bf16[1024,256]{1,0:T(8,128)(2,1)S(1)}, bf16[1024,256]{1,0:T(8,128)(2,1)}, u32[]{:S(2)}) copy-start(bf16[1024,256]{1,0:T(8,128)(2,1)} %param.14) | copy-start | bytes 1572868
  12.1 1.1 copy-start.1
  12.1 1.1 copy-start.2

commit v2 on v1

v2 whole, which is shorter than its diff:
```python
import functools

import jax
import jax.numpy as jnp
from jax import lax
from jax.experimental import pallas as pl
from jax.experimental.pallas import tpu as pltpu
from jax.sharding import PartitionSpec as P

MESH = pl.DeviceIdType.MESH
F32 = jnp.float32
BF16 = jnp.bfloat16

LEN = 128
EPSILON = 1e-06
GATE_EXPONENT = 8.0

SIDE = 4
CHUNKS = 4
ROWS = 1024
CH = ROWS // CHUNKS
HALF = CH // 2
STEPS = LEN // CHUNKS
SEQS = 8
R = 352
RP = 384
FFL = 704
FP = 768
CB = 256
NT = (((1,), (1,)), ((), ()))

WGI_ROWS = (((0, 176), (176, 176)), ((RP, 176), (RP + 176, 176)))
WO_ROWS = (((0, 96), (96, 80)), ((176, 96), (272, 80)))
WFF_ROWS = (((0, 352), (352, 352)), ((FP, 352), (FP + 352, 352)))
WD_ROWS = (((0, 176), (176, 176)), ((352, 176), (528, 176)))


class Gather:
    def __init__(self, buf, rows, send, recv, pos, dev):
        self.buf, self.rows, self.send, self.recv, self.dev = buf, rows, send, recv, dev
        self.axes = (("x", "z"), ("z", "x"))
        self.pos = pos

    def block(self, part, i1, i2, half=None):
        z, x = (i2, i1) if part == 0 else (i1, i2)
        lo, hi = self.rows[part]
        span = pl.ds(lo[0], lo[1] + hi[1]) if half is None else pl.ds(*(lo, hi)[half])
        return self.buf.at[span, pl.ds(pl.multiple_of((z * SIDE + x) * 128, 128), 128)]

    def copy(self, view, part, k, to):
        return pltpu.make_async_remote_copy(
            src_ref=view,
            dst_ref=view,
            send_sem=self.send.at[part, k],
            recv_sem=self.recv.at[part, k],
            device_id=to,
            device_id_type=MESH,
        )

    def places(self, part):
        a1, a2 = self.axes[part]
        (m1, i1, p1), (m2, i2, p2) = self.pos[a1], self.pos[a2]
        far1, far2 = lax.rem(i1 + 2, SIDE), lax.rem(i2 + 2, SIDE)
        return (i1, m1, p1, far1), (i2, m2, p2, far2), self.dev[a1], self.dev[a2]

    def landing(self, part, k):
        first, second, _, _ = self.places(part)
        if k < 4:
            where = (first[1], first[2], first[3], first[3])[k]
            return self.block(part, where, second[0], None if k < 2 else k - 2)
        q, k = divmod(k - 4, 4)
        where = (second[1], second[2], second[3], second[3])[k]
        return self.block(part, first[q], where, None if k < 2 else k - 2)

    def arrived(self, part, k):
        self.copy(self.landing(part, k), part, k, self.dev["x"][0]).wait_recv()

    def onto_second(self, part, q):
        first, second, _, dev2 = self.places(part)
        view = self.block(part, first[q], second[0])
        self.copy(view, part, 4 + 4 * q, dev2[1]).start()
        self.copy(view, part, 5 + 4 * q, dev2[0]).start()

    def own(self):
        for part in (0, 1):
            first, second, dev1, _ = self.places(part)
            view = self.block(part, first[0], second[0])
            self.copy(view, part, 0, dev1[1]).start()
            self.copy(view, part, 1, dev1[0]).start()
        for part in (0, 1):
            self.onto_second(part, 0)

    def near(self):
        for part in (0, 1):
            first, second, dev1, _ = self.places(part)
            self.arrived(part, 0)
            self.copy(self.block(part, first[1], second[0], 0), part, 2, dev1[1]).start()
            self.arrived(part, 1)
            self.copy(self.block(part, first[2], second[0], 1), part, 3, dev1[0]).start()
        for part in (0, 1):
            self.onto_second(part, 1)
            self.onto_second(part, 2)

    def far(self):
        for part in (0, 1):
            self.arrived(part, 2)
            self.arrived(part, 3)
            self.onto_second(part, 3)

    def relay(self, q):
        for part in (0, 1):
            first, second, _, dev2 = self.places(part)
            self.arrived(part, 4 + 4 * q)
            self.copy(self.block(part, first[q], second[1], 0), part, 6 + 4 * q, dev2[1]).start()
            self.arrived(part, 5 + 4 * q)
            self.copy(self.block(part, first[q], second[2], 1), part, 7 + 4 * q, dev2[0]).start()

    def done(self):
        for part in (0, 1):
            for q in range(4):
                self.arrived(part, 6 + 4 * q)
                self.arrived(part, 7 + 4 * q)

    def drain(self):
        for part in (0, 1):
            for k in range(20):
                self.copy(self.landing(part, k), part, k, self.dev["x"][0]).wait_send()


class Spread:
    def __init__(self, buf, send, recv, y, core, dev):
        self.buf, self.send, self.recv, self.dev = buf, send, recv, dev
        (ym, yy, yp), far = y, lax.rem(y[1] + 2, SIDE)
        other = 1 - core
        self.own, self.minus, self.plus, self.far = (2 * v + core for v in (yy, ym, yp, far))
        self.others = [2 * v + other for v in (yy, ym, yp, far)]

    def view(self, block, c, half=None):
        if half is None:
            return self.buf.at[block, pl.ds(pl.multiple_of(c * CH, CH), CH), :]
        return self.buf.at[block, pl.ds(pl.multiple_of(c * CH + half * HALF, HALF), HALF), :]

    def copy(self, view, k, c, to):
        return pltpu.make_async_remote_copy(
            src_ref=view,
            dst_ref=view,
            send_sem=self.send.at[k, c],
            recv_sem=self.recv.at[k, c],
            device_id=to,
            device_id_type=MESH,
        )

    def landing(self, k, c):
        return [
            (self.minus, None),
            (self.plus, None),
            (self.others[0], None),
            (self.far, 0),
            (self.far, 1),
            (self.others[1], None),
            (self.others[2], None),
            (self.others[3], None),
        ][k]

    def arrived(self, k, c):
        block, half = self.landing(k, c)
        self.copy(self.view(block, c, half), k, c, self.dev["core"]).wait_recv()

    def stage0(self, c):
        view = self.view(self.own, c)
        self.copy(view, 0, c, self.dev["y"][1]).start()
        self.copy(view, 1, c, self.dev["y"][0]).start()
        self.copy(view, 2, c, self.dev["core"]).start()

    def stage1(self, c):
        self.arrived(0, c)
        self.copy(self.view(self.minus, c, 0), 3, c, self.dev["y"][1]).start()
        self.copy(self.view(self.minus, c), 5, c, self.dev["core"]).start()
        self.arrived(1, c)
        self.copy(self.view(self.plus, c, 1), 4, c, self.dev["y"][0]).start()
        self.copy(self.view(self.plus, c), 6, c, self.dev["core"]).start()

    def stage2(self, c):
        self.arrived(3, c)
        self.arrived(4, c)
        self.copy(self.view(self.far, c), 7, c, self.dev["core"]).start()

    def stage3(self, c):
        for k in (2, 5, 6, 7):
            self.arrived(k, c)

    def drain(self, c):
        for k in range(8):
            block, half = self.landing(k, c)
            self.copy(self.view(block, c, half), k, c, self.dev["core"]).wait_send()


class Sum:
    def __init__(self, part, took, total, halves, finals, send, recv, y, core, dev):
        self.part, self.took, self.total = part, took, total
        self.halves, self.finals, self.send, self.recv, self.dev = halves, finals, send, recv, dev
        self.minus, self.own, self.plus = y
        self.far = lax.rem(y[1] + 2, SIDE)
        self.core = core

    def rows(self, c):
        return pl.ds(pl.multiple_of(c * CH, CH), CH)

    def half(self, c, h):
        return pl.ds(pl.multiple_of(c * CH + h * HALF, HALF), HALF)

    def parts(self, k, c):
        if k == 0:
            return self.part.at[:, 1 - self.core, self.rows(c), :], self.took.at[:, self.rows(c), :], self.dev["core"]
        if k <= 2:
            return self.total.at[self.far, self.half(c, k - 1), :], self.halves.at[k - 1, c], self.dev["y"][2 - k]
        to = self.plus if k == 3 else self.minus
        return self.total.at[to, self.rows(c), :], self.finals.at[k - 3, self.rows(c), :], self.dev["y"][4 - k]

    def copy(self, k, c):
        src, dst, to = self.parts(k, c)
        return pltpu.make_async_remote_copy(
            src_ref=src,
            dst_ref=dst,
            send_sem=self.send.at[k, c],
            recv_sem=self.recv.at[k, c],
            device_id=to,
            device_id_type=MESH,
        )

    def stage0(self, c):
        self.copy(0, c).start()

    def stage1(self, c):
        self.copy(0, c).wait_recv()
        rows = self.rows(c)

        def add(target):
            self.total[target, rows, :] = (
                self.part[target, self.core, rows, :].astype(F32) + self.took[target, rows, :].astype(F32)
            ).astype(BF16)

        add(self.far)
        add(self.plus)
        self.copy(1, c).start()
        self.copy(2, c).start()
        add(self.minus)
        add(self.own)

    def stage2(self, c):
        for h, target in ((0, self.plus), (1, self.minus)):
            self.copy(1 + h, c).wait_recv()
            rows = self.half(c, h)
            self.total[target, rows, :] = (
                self.total[target, rows, :].astype(F32) + self.halves[h, c].astype(F32)
            ).astype(BF16)
        self.copy(3, c).start()
        self.copy(4, c).start()

    def stage3(self, c):
        self.copy(3, c).wait_recv()
        self.copy(4, c).wait_recv()
        rows = self.rows(c)
        return (
            self.total[self.own, rows, :].astype(F32)
            + self.finals[0, rows, :].astype(F32)
            + self.finals[1, rows, :].astype(F32)
        )

    def drain(self, c):
        for k in range(5):
            self.copy(k, c).wait_send()


def norm_chunk(full, gain, out, c):
    step = 16

    def body(i, carry):
        rows = pl.ds(pl.multiple_of(c * CH + i * step, step), step)
        here = pl.ds(pl.multiple_of(i * step, step), step)
        total = jnp.zeros((step, CB), F32)
        for b in range(8):
            v = full[b, rows, :].astype(F32)
            total = total + v * v
        scale = lax.rsqrt(jnp.sum(total, axis=1, keepdims=True) * (1.0 / 2048.0) + EPSILON)
        for b in range(8):
            v = full[b, rows, :].astype(F32) * scale
            for s in range(2):
                g = gain[2 * b + s : 2 * b + s + 1, :]
                lo = b * CB + s * 128
                out[here, lo : lo + 128] = (v[:, s * 128 : s * 128 + 128] * g).astype(BF16)
        return carry

    lax.fori_loop(0, CH // step, body, 0, unroll=2)


def order(shape, major):
    to = lax.broadcasted_iota(jnp.int32, shape, 0)
    source = lax.broadcasted_iota(jnp.int32, shape, 1)
    if major == "time":
        wanted = lax.rem(to, SEQS) * STEPS + to // SEQS
    else:
        wanted = lax.rem(to, STEPS) * SEQS + to // STEPS
    return jnp.where(source == wanted, 1.0, 0.0).astype(BF16)


def kernel(
    wg_hbm, wi_hbm, tok_hbm, wo_hbm, wfg_hbm, wfu_hbm, wd_hbm,
    gr_hbm, gi_hbm, taps_hbm, base_hbm, ld_hbm, gain1_hbm, gain2_hbm,
    out,
    full1, full2, wgi, wo, wff, wd,
    part1, took1, total1, halves1, finals1,
    part2, took2, total2, halves2, finals2,
    tokv, grv, giv, tapsv, basev, ldv, gain1, gain2,
    gm, small, ldb, perm,
    feat, proj, mixed, gl, carried, nrm, ffo, hid, state,
    local_sem, w_send, w_recv, a_send, a_recv, s_send, s_recv,
):
    fs, tp = lax.axis_index("fs"), lax.axis_index("tp")
    iz, ix = fs // SIDE, lax.rem(fs, SIDE)
    iy, core = tp // 2, lax.rem(tp, 2)

    def ring(i):
        return lax.rem(i + SIDE - 1, SIDE), i, lax.rem(i + 1, SIDE)

    pos = {"x": ring(ix), "z": ring(iz)}
    y = ring(iy)
    dev = {
        "x": tuple({"fs": iz * SIDE + pos["x"][k]} for k in (0, 2)),
        "z": tuple({"fs": pos["z"][k] * SIDE + ix} for k in (0, 2)),
        "y": tuple({"tp": 2 * y[k] + core} for k in (0, 2)),
        "core": {"tp": 2 * iy + 1 - core},
    }

    barrier = pltpu.get_barrier_semaphore()
    for to in (*dev["x"], *dev["z"], *dev["y"], dev["core"]):
        pl.semaphore_signal(barrier, inc=1, device_id=to, device_id_type=MESH)

    cols = pl.ds(pl.multiple_of(fs * 128, 128), 128)
    local = [
        pltpu.make_async_copy(src, dst, local_sem.at[n])
        for n, (src, dst) in enumerate(
            (
                (wg_hbm, wgi.at[pl.ds(0, R), cols]),
                (wi_hbm, wgi.at[pl.ds(RP, R), cols]),
                (tok_hbm, tokv),
                (wo_hbm, wo.at[pl.ds(0, R), cols]),
                (wfg_hbm, wff.at[pl.ds(0, FFL), cols]),
                (wfu_hbm, wff.at[pl.ds(FP, FFL), cols]),
                (wd_hbm, wd.at[:, cols]),
                (gr_hbm, grv),
                (gi_hbm, giv),
                (taps_hbm, tapsv),
                (base_hbm, basev),
                (ld_hbm, ldv),
                (gain1_hbm, gain1),
                (gain2_hbm, gain2),
            )
        )
    ]
    for copy in local:
        copy.start()
    wgi[R:RP, :] = jnp.zeros((RP - R, 2048), BF16)
    wgi[RP + R :, :] = jnp.zeros((RP - R, 2048), BF16)
    wo[R:RP, :] = jnp.zeros((RP - R, 2048), BF16)
    wff[FFL:FP, :] = jnp.zeros((FP - FFL, 2048), BF16)
    perm[...] = order((CH, CH), "time")

    gathers = [
        Gather(buf, rows, w_send.at[m], w_recv.at[m], pos, dev)
        for m, (buf, rows) in enumerate(((wgi, WGI_ROWS), (wo, WO_ROWS), (wff, WFF_ROWS), (wd, WD_ROWS)))
    ]
    g_wgi, g_wo, g_wff, g_wd = gathers
    spread1 = Spread(full1, a_send.at[0], a_recv.at[0], y, core, dev)
    spread2 = Spread(full2, a_send.at[1], a_recv.at[1], y, core, dev)
    sum1 = Sum(part1, took1, total1, halves1, finals1, s_send.at[0], s_recv.at[0], y, core, dev)
    sum2 = Sum(part2, took2, total2, halves2, finals2, s_send.at[1], s_recv.at[1], y, core, dev)

    def reordered(c):
        pieces = [tokv[s * LEN + c * STEPS : s * LEN + (c + 1) * STEPS, :] for s in range(SEQS)]
        full1[tp, c * CH : (c + 1) * CH, :] = jnp.dot(
            perm[...], jnp.concatenate(pieces, axis=0), preferred_element_type=F32
        ).astype(BF16)

    local[2].wait()
    for c in range(CHUNKS):
        reordered(c)
    local[0].wait()
    local[1].wait()
    pl.semaphore_wait(barrier, 7)

    g_wgi.own()
    for c in range(CHUNKS):
        spread1.stage0(c)
    local[3].wait()
    g_wo.own()

    for n in range(7, 14):
        local[n].wait()
    gm[...] = jnp.zeros_like(gm)
    gm[0:R, 0:R] = grv[...]
    gm[0:R, RP : RP + R] = giv[...]
    small[...] = jnp.zeros_like(small)
    small[0:4, 0:R] = tapsv[...]
    small[4:5, 0:R] = -GATE_EXPONENT * jax.nn.softplus(-basev[...])
    for t in range(LEN):
        ldb[8 * t : 8 * t + 8, :] = jnp.broadcast_to(ldv[:, t : t + 1], (SEQS, 128))
    feat[0:24, :] = jnp.zeros((24, RP), F32)
    state[...] = jnp.zeros_like(state)
    for n in range(4, 7):
        local[n].wait()

    g_wgi.near()
    spread1.stage1(0)
    g_wgi.relay(0)
    g_wo.near()
    spread1.stage1(1)
    g_wgi.far()
    g_wgi.relay(1)
    spread1.stage1(2)
    g_wo.relay(0)
    g_wgi.relay(2)
    g_wo.far()
    spread1.stage1(3)
    spread1.stage2(0)
    g_wo.relay(1)
    spread1.stage2(1)
    g_wgi.relay(3)
    g_wo.relay(2)
    g_wo.relay(3)
    g_wff.own()
    spread1.stage2(2)
    spread1.stage2(3)

    def mix_in(c):
        spread1.stage3(c)
        norm_chunk(full1, gain1, nrm, c)
        base = pl.multiple_of(c * CH, CH)

        @pl.when(c == 0)
        def _():
            g_wgi.done()

        projected = lax.dot_general(nrm[...], wgi[...], NT, preferred_element_type=F32)
        proj[...] = projected[:, :RP]
        feat[pl.ds(base + 24, CH), :] = projected[:, RP:].astype(BF16).astype(F32)

    def mix_out(c):
        base = pl.multiple_of(c * CH, CH)

        def taps(i, carry):
            r = pl.multiple_of(i * 32, 32)
            summed = small[0:1, :] * feat[pl.ds(base + r, 32), :]
            for k in range(1, 4):
                summed = summed + small[k : k + 1, :] * feat[pl.ds(base + r + 8 * k, 32), :]
            mixed[pl.ds(r, 32), :] = summed.astype(BF16)
            return carry

        lax.fori_loop(0, CH // 32, taps, 0, unroll=2)
        gl[...] = jnp.dot(mixed[...], gm[...], preferred_element_type=F32)

        def steps(i, h):
            r = pl.multiple_of(i * 32, 32)
            rows = pl.ds(r, 32)
            recur = jax.nn.sigmoid(gl[rows, :RP])
            inject = jax.nn.sigmoid(gl[rows, RP:])
            struck = ldb[pl.ds(base + r, 32), :]
            log_decay = small[4:5, :] * recur + jnp.concatenate([struck] * 3, axis=1)
            decay = jnp.exp(log_decay)
            twice = 2.0 * log_decay
            near = -twice * (1.0 + twice * (0.5 + twice * (1.0 / 6.0 + twice * (1.0 / 24.0 + twice * (1.0 / 120.0)))))
            rest = jnp.where(twice > -0.1, near, 1.0 - decay * decay)
            driven = jnp.sqrt(rest) * (inject * mixed[rows, :].astype(F32))
            states = []
            for s in range(4):
                h = decay[8 * s : 8 * s + 8] * h + driven[8 * s : 8 * s + 8]
                states.append(h)
            carried[rows, :] = (jnp.concatenate(states, axis=0) * jax.nn.gelu(proj[rows, :])).astype(BF16)
            return h

        state[...] = lax.fori_loop(0, CH // 32, steps, state[...])

        @pl.when(c == 0)
        def _():
            g_wo.done()

        rows = pl.ds(base, CH)
        for j in range(8):
            part1[j // 2, j % 2, rows, :] = jnp.dot(
                carried[...], wo[:, j * CB : (j + 1) * CB], preferred_element_type=F32
            ).astype(BF16)
        sum1.stage0(c)

    def settle(c):
        rows = pl.ds(pl.multiple_of(c * CH, CH), CH)
        full2[tp, rows, :] = (full1[tp, rows, :].astype(F32) + sum1.stage3(c)).astype(BF16)
        spread2.stage0(c)

    def up(c):
        spread2.stage3(c)
        norm_chunk(full2, gain2, nrm, c)

        @pl.when(c == 0)
        def _():
            g_wff.done()

        ffo[...] = lax.dot_general(nrm[...], wff[...], NT, preferred_element_type=F32)
        base = pl.multiple_of(c * CH, CH)

        def act(i, carry):
            r = pl.multiple_of(i * 16, 16)
            rows = pl.ds(r, 16)
            hid[pl.ds(base + r, 16), :] = (jax.nn.silu(ffo[rows, :FFL]) * ffo[rows, FP:]).astype(BF16)
            return carry

        lax.fori_loop(0, CH // 16, act, 0, unroll=2)

    def down(c):
        @pl.when(c == 0)
        def _():
            g_wd.done()

        rows = pl.ds(pl.multiple_of(c * CH, CH), CH)
        for j in range(8):
            part2[j // 2, j % 2, rows, :] = jnp.dot(
                hid[rows, :], wd[:, j * CB : (j + 1) * CB], preferred_element_type=F32
            ).astype(BF16)
        sum2.stage0(c)

    def finish(c):
        rows = pl.ds(pl.multiple_of(c * CH, CH), CH)
        layer_out = (full2[tp, rows, :].astype(F32) + sum2.stage3(c)).astype(BF16)
        ordered = jnp.dot(perm[...], layer_out, preferred_element_type=F32).astype(BF16)
        for s in range(SEQS):
            out[pl.ds(pl.multiple_of(s * LEN + c * STEPS, STEPS), STEPS), :] = ordered[s * STEPS : (s + 1) * STEPS]

    def turn(c):
        @pl.when(c == 0)
        def _():
            perm[...] = order((CH, CH), "sequence")

    events = {
        0: (g_wff.near,),
        1: (functools.partial(g_wff.relay, 0), g_wff.far),
        2: (functools.partial(g_wff.relay, 1), g_wd.own),
        3: (functools.partial(g_wff.relay, 2),),
        4: (functools.partial(g_wff.relay, 3),),
        5: (g_wd.near,),
        6: (functools.partial(g_wd.relay, 0),),
        7: (g_wd.far,),
        8: (functools.partial(g_wd.relay, 1),),
        9: (functools.partial(g_wd.relay, 2), functools.partial(g_wd.relay, 3)),
    }

    def weights(i):
        for when, calls in events.items():

            @pl.when(i == when)
            def _():
                for call in calls:
                    call()

    stages = [
        (0, mix_in),
        (1, sum1.stage1),
        (2, sum1.stage2),
        (3, settle),
        (0, mix_out),
        (4, spread2.stage1),
        (5, spread2.stage2),
        (None, weights),
        (4, turn),
        (6, up),
        (11, sum2.stage1),
        (10, down),
        (14, sum2.stage2),
        (16, finish),
    ]

    def tick(i, carry):
        for lag, stage in stages:
            if lag is None:
                stage(i)
            else:
                pl.when((i >= lag) & (i < lag + CHUNKS))(functools.partial(stage, i - lag))
        return carry

    lax.fori_loop(0, CHUNKS + 16, tick, 0)

    for gather in gathers:
        gather.drain()

    def drained(c, carry):
        for group in (spread1, spread2, sum1, sum2):
            group.drain(c)
        return carry

    lax.fori_loop(0, CHUNKS, drained, 0)


def layer(*operands):
    sums = [
        pltpu.VMEM((SIDE, 2, ROWS, CB), BF16),
        pltpu.VMEM((SIDE, ROWS, CB), BF16),
        pltpu.VMEM((SIDE, ROWS, CB), BF16),
        pltpu.VMEM((2, CHUNKS, HALF, CB), BF16),
        pltpu.VMEM((2, ROWS, CB), BF16),
    ]
    return pl.pallas_call(
        kernel,
        out_shape=jax.ShapeDtypeStruct((ROWS, CB), BF16),
        in_specs=[pl.BlockSpec(memory_space=pl.ANY)] * len(operands),
        out_specs=pl.BlockSpec(memory_space=pltpu.VMEM),
        scratch_shapes=[
            pltpu.VMEM((8, ROWS, CB), BF16),
            pltpu.VMEM((8, ROWS, CB), BF16),
            pltpu.VMEM((2 * RP, 2048), BF16),
            pltpu.VMEM((RP, 2048), BF16),
            pltpu.VMEM((FP + FFL, 2048), BF16),
            pltpu.VMEM((FFL, 2048), BF16),
            *sums,
            *sums,
            pltpu.VMEM((ROWS, CB), BF16),
            pltpu.VMEM((R, R), BF16),
            pltpu.VMEM((R, R), BF16),
            pltpu.VMEM((4, R), F32),
            pltpu.VMEM((1, R), F32),
            pltpu.VMEM((SEQS, LEN), F32),
            pltpu.VMEM((16, 128), F32),
            pltpu.VMEM((16, 128), F32),
            pltpu.VMEM((RP, 2 * RP), BF16),
            pltpu.VMEM((8, RP), F32),
            pltpu.VMEM((ROWS, 128), F32),
            pltpu.VMEM((CH, CH), BF16),
            pltpu.VMEM((24 + ROWS, RP), F32),
            pltpu.VMEM((CH, RP), F32),
            pltpu.VMEM((CH, RP), BF16),
            pltpu.VMEM((CH, 2 * RP), F32),
            pltpu.VMEM((CH, RP), BF16),
            pltpu.VMEM((CH, 2048), BF16),
            pltpu.VMEM((CH, FP + FFL), F32),
            pltpu.VMEM((ROWS, FFL), BF16),
            pltpu.VMEM((SEQS, RP), F32),
            pltpu.SemaphoreType.DMA((14,)),
            pltpu.SemaphoreType.DMA((4, 2, 20)),
            pltpu.SemaphoreType.DMA((4, 2, 20)),
            pltpu.SemaphoreType.DMA((2, 8, CHUNKS)),
            pltpu.SemaphoreType.DMA((2, 8, CHUNKS)),
            pltpu.SemaphoreType.DMA((2, 5, CHUNKS)),
            pltpu.SemaphoreType.DMA((2, 5, CHUNKS)),
        ],
        compiler_params=pltpu.CompilerParams(
            collective_id=0, has_side_effects=True, vmem_limit_bytes=66_000_000
        ),
    )(*operands)


def shards(
    tokens,
    recurrence_norm_gain,
    output_gate_weight,
    recurrence_input_weight,
    convolution_taps,
    recurrence_gate_weight,
    input_gate_weight,
    base_decay_logit,
    token_log_decay,
    recurrence_output_weight,
    feedforward_norm_gain,
    feedforward_gate_weight,
    feedforward_up_weight,
    feedforward_down_weight,
):
    return layer(
        output_gate_weight.T,
        recurrence_input_weight.T,
        tokens,
        recurrence_output_weight,
        feedforward_gate_weight.T,
        feedforward_up_weight.T,
        feedforward_down_weight,
        recurrence_gate_weight.reshape(R, R),
        input_gate_weight.reshape(R, R),
        convolution_taps,
        base_decay_logit.reshape(1, R),
        token_log_decay.reshape(SEQS, LEN),
        recurrence_norm_gain.reshape(16, 128),
        feedforward_norm_gain.reshape(16, 128),
    )


def solution(mesh):
    in_specs = (
        P("fs", "tp"),
        P(),
        P("fs", "tp"),
        P("fs", "tp"),
        P(None, "tp"),
        P("tp", None, None),
        P("tp", None, None),
        P("tp"),
        P("fs"),
        P("tp", "fs"),
        P(),
        P("fs", "tp"),
        P("fs", "tp"),
        P("tp", "fs"),
    )
    return jax.shard_map(shards, mesh=mesh, in_specs=in_specs, out_specs=P("fs", "tp"), check_vma=False)
```

time: 170 us -> 124 us (0.73)
  Pallas kernels: 154 us -> 120 us
  local copies, waits for them, and re-layouts: 12.4 us -> 3.11 us
  other arithmetic: 3.6 us -> 0 us
    pallas_call x1, Pallas kernels: 154 us -> 120 us  [layer(): pl.pallas_call(kernel, out_shape=jax.ShapeDtypeStruct((ROWS, CB), BF16),...]
    reshape x4 -> x1, local copies, waits for them, and re-layouts: 4.64 us -> 0.56 us  [shards(): base_decay_logit.reshape(1, R)]
    concatenate x3 -> x0, other arithmetic: 2.91 us -> none  [the longest x1 1.3 us: shards(): jnp.concatenate([convolution_taps, rate[None, :]], axis=0)]
    transpose x2 -> x0, local copies, waits for them, and re-layouts: 2.77 us -> none  [the longest x1 1.94 us: shards(): return out.reshape(LEN, SEQS, CB).transpose(1, 0, 2).reshape(ROWS, CB)]
where the time goes in v2:
time: 124 us; the launch traced here: 123 us
  Pallas kernels  120 us (97%)
  local copies, waits for them, and re-layouts  3.11 us (3%)
    pallas_call x1, Pallas kernels, layer(): pl.pallas_call(kernel, out_shape=jax.ShapeDtypeStruct((ROWS, CB), BF16),...  120 us
    unnamed x3, local copies, waits for them, and re-layouts  2.55 us

profile of v2, /device:TPU:1, one launch (start us, length us, event | category | flops | bytes accessed | tf_op | source)
XLA Modules:
  0.0 123.4 jit_solution(6215783170792553252)
XLA Ops:
  0.0 0.0 copy-start
  0.0 0.7 copy-done
  0.7 0.6 reshape.20.base_hbm
  1.2 120.3 %shard_map.136 = bf16[1024,256]{1,0:T(8,128)(2,1)} custom-call(bf16[352,128]{1,0:T(8,128)(2,1)} %bitcast.13, bf16[352,128]{1,0:T(8,128)(2,1)} %bitcast.14, bf16[1024,256]{1,0:T(8,128)(2,1)} %tok_hbm.1, bf16[352,128]{1,0:T(8,128)(2,1)} %wo_hbm.1, bf16[704,128]{1,0:T(8,128)(2,1)} %bitcast.11, bf16[704,128]{1,0:T(8,128)(2,1)} %bitcast.12, ...), custom_call_target="tpu_custom_call" | custom-call | tf_op jit(solution)/shard_map/pallas_call | solution.py:609
  121.5 1.9 %copy.16 = bf16[1024,256]{1,0:T(8,128)(2,1)} copy(bf16[1024,256]{1,0:T(8,128)(2,1)} %shard_map.136) | data formatting | bytes 1048576
Async XLA Ops:
  0.0 0.7 copy-start

commit v3 on v2

--- a/solution.py
+++ b/solution.py
@@ -1,5 +1,3 @@
-import functools
-
 import jax
 import jax.numpy as jnp
 from jax import lax
@@ -137,8 +135,8 @@
 
     def view(self, block, c, half=None):
         if half is None:
-            return self.buf.at[block, pl.ds(pl.multiple_of(c * CH, CH), CH), :]
-        return self.buf.at[block, pl.ds(pl.multiple_of(c * CH + half * HALF, HALF), HALF), :]
+            return self.buf.at[block, pl.ds(c * CH, CH), :]
+        return self.buf.at[block, pl.ds(c * CH + half * HALF, HALF), :]
 
     def copy(self, view, k, c, to):
         return pltpu.make_async_remote_copy(
@@ -204,10 +202,10 @@
         self.core = core
 
     def rows(self, c):
-        return pl.ds(pl.multiple_of(c * CH, CH), CH)
+        return pl.ds(c * CH, CH)
 
     def half(self, c, h):
-        return pl.ds(pl.multiple_of(c * CH + h * HALF, HALF), HALF)
+        return pl.ds(c * CH + h * HALF, HALF)
 
     def parts(self, k, c):
         if k == 0:
@@ -389,64 +387,32 @@
     local[1].wait()
     pl.semaphore_wait(barrier, 7)
 
-    g_wgi.own()
-    for c in range(CHUNKS):
-        spread1.stage0(c)
-    local[3].wait()
-    g_wo.own()
-
-    for n in range(7, 14):
-        local[n].wait()
-    gm[...] = jnp.zeros_like(gm)
-    gm[0:R, 0:R] = grv[...]
-    gm[0:R, RP : RP + R] = giv[...]
-    small[...] = jnp.zeros_like(small)
-    small[0:4, 0:R] = tapsv[...]
-    small[4:5, 0:R] = -GATE_EXPONENT * jax.nn.softplus(-basev[...])
-    for t in range(LEN):
-        ldb[8 * t : 8 * t + 8, :] = jnp.broadcast_to(ldv[:, t : t + 1], (SEQS, 128))
-    feat[0:24, :] = jnp.zeros((24, RP), F32)
-    state[...] = jnp.zeros_like(state)
-    for n in range(4, 7):
-        local[n].wait()
-
-    g_wgi.near()
-    spread1.stage1(0)
-    g_wgi.relay(0)
-    g_wo.near()
-    spread1.stage1(1)
-    g_wgi.far()
-    g_wgi.relay(1)
-    spread1.stage1(2)
-    g_wo.relay(0)
-    g_wgi.relay(2)
-    g_wo.far()
-    spread1.stage1(3)
-    spread1.stage2(0)
-    g_wo.relay(1)
-    spread1.stage2(1)
-    g_wgi.relay(3)
-    g_wo.relay(2)
-    g_wo.relay(3)
-    g_wff.own()
-    spread1.stage2(2)
-    spread1.stage2(3)
-
-    def mix_in(c):
+    def small_operands():
+        for n in range(7, 14):
+            local[n].wait()
+        gm[...] = jnp.zeros_like(gm)
+        gm[0:R, 0:R] = grv[...]
+        gm[0:R, RP : RP + R] = giv[...]
+        small[...] = jnp.zeros_like(small)
+        small[0:4, 0:R] = tapsv[...]
+        small[4:5, 0:R] = -GATE_EXPONENT * jax.nn.softplus(-basev[...])
+        for t in range(LEN):
+            ldb[8 * t : 8 * t + 8, :] = jnp.broadcast_to(ldv[:, t : t + 1], (SEQS, 128))
+        feat[0:24, :] = jnp.zeros((24, RP), F32)
+        state[...] = jnp.zeros_like(state)
+
+    def norm1(c):
         spread1.stage3(c)
         norm_chunk(full1, gain1, nrm, c)
-        base = pl.multiple_of(c * CH, CH)
-
-        @pl.when(c == 0)
-        def _():
-            g_wgi.done()
-
+
+    def project(c):
+        base = c * CH
         projected = lax.dot_general(nrm[...], wgi[...], NT, preferred_element_type=F32)
         proj[...] = projected[:, :RP]
         feat[pl.ds(base + 24, CH), :] = projected[:, RP:].astype(BF16).astype(F32)
 
-    def mix_out(c):
-        base = pl.multiple_of(c * CH, CH)
+    def scan(c):
+        base = c * CH
 
         def taps(i, carry):
             r = pl.multiple_of(i * 32, 32)
@@ -480,11 +446,8 @@
 
         state[...] = lax.fori_loop(0, CH // 32, steps, state[...])
 
-        @pl.when(c == 0)
-        def _():
-            g_wo.done()
-
-        rows = pl.ds(base, CH)
+    def mix_out(c):
+        rows = pl.ds(c * CH, CH)
         for j in range(8):
             part1[j // 2, j % 2, rows, :] = jnp.dot(
                 carried[...], wo[:, j * CB : (j + 1) * CB], preferred_element_type=F32
@@ -492,35 +455,30 @@
         sum1.stage0(c)
 
     def settle(c):
-        rows = pl.ds(pl.multiple_of(c * CH, CH), CH)
+        rows = pl.ds(c * CH, CH)
         full2[tp, rows, :] = (full1[tp, rows, :].astype(F32) + sum1.stage3(c)).astype(BF16)
         spread2.stage0(c)
 
-    def up(c):
+    def norm2(c):
         spread2.stage3(c)
         norm_chunk(full2, gain2, nrm, c)
 
-        @pl.when(c == 0)
-        def _():
-            g_wff.done()
-
+    def up(c):
         ffo[...] = lax.dot_general(nrm[...], wff[...], NT, preferred_element_type=F32)
-        base = pl.multiple_of(c * CH, CH)
-
-        def act(i, carry):
+
+    def act(c):
+        base = c * CH
+
+        def body(i, carry):
             r = pl.multiple_of(i * 16, 16)
             rows = pl.ds(r, 16)
             hid[pl.ds(base + r, 16), :] = (jax.nn.silu(ffo[rows, :FFL]) * ffo[rows, FP:]).astype(BF16)
             return carry
 
-        lax.fori_loop(0, CH // 16, act, 0, unroll=2)
+        lax.fori_loop(0, CH // 16, body, 0, unroll=2)
 
     def down(c):
-        @pl.when(c == 0)
-        def _():
-            g_wd.done()
-
-        rows = pl.ds(pl.multiple_of(c * CH, CH), CH)
+        rows = pl.ds(c * CH, CH)
         for j in range(8):
             part2[j // 2, j % 2, rows, :] = jnp.dot(
                 hid[rows, :], wd[:, j * CB : (j + 1) * CB], preferred_element_type=F32
@@ -528,74 +486,133 @@
         sum2.stage0(c)
 
     def finish(c):
-        rows = pl.ds(pl.multiple_of(c * CH, CH), CH)
+        rows = pl.ds(c * CH, CH)
         layer_out = (full2[tp, rows, :].astype(F32) + sum2.stage3(c)).astype(BF16)
         ordered = jnp.dot(perm[...], layer_out, preferred_element_type=F32).astype(BF16)
         for s in range(SEQS):
-            out[pl.ds(pl.multiple_of(s * LEN + c * STEPS, STEPS), STEPS), :] = ordered[s * STEPS : (s + 1) * STEPS]
-
-    def turn(c):
-        @pl.when(c == 0)
-        def _():
-            perm[...] = order((CH, CH), "sequence")
-
-    events = {
-        0: (g_wff.near,),
-        1: (functools.partial(g_wff.relay, 0), g_wff.far),
-        2: (functools.partial(g_wff.relay, 1), g_wd.own),
-        3: (functools.partial(g_wff.relay, 2),),
-        4: (functools.partial(g_wff.relay, 3),),
-        5: (g_wd.near,),
-        6: (functools.partial(g_wd.relay, 0),),
-        7: (g_wd.far,),
-        8: (functools.partial(g_wd.relay, 1),),
-        9: (functools.partial(g_wd.relay, 2), functools.partial(g_wd.relay, 3)),
-    }
-
-    def weights(i):
-        for when, calls in events.items():
-
-            @pl.when(i == when)
-            def _():
-                for call in calls:
-                    call()
-
-    stages = [
-        (0, mix_in),
-        (1, sum1.stage1),
-        (2, sum1.stage2),
-        (3, settle),
-        (0, mix_out),
-        (4, spread2.stage1),
-        (5, spread2.stage2),
-        (None, weights),
-        (4, turn),
-        (6, up),
-        (11, sum2.stage1),
-        (10, down),
-        (14, sum2.stage2),
-        (16, finish),
-    ]
-
-    def tick(i, carry):
-        for lag, stage in stages:
-            if lag is None:
-                stage(i)
-            else:
-                pl.when((i >= lag) & (i < lag + CHUNKS))(functools.partial(stage, i - lag))
-        return carry
-
-    lax.fori_loop(0, CHUNKS + 16, tick, 0)
+            out[pl.ds(s * LEN + c * STEPS, STEPS), :] = ordered[s * STEPS : (s + 1) * STEPS]
+
+    g_wgi.own()
+    spread1.stage0(0)
+    local[3].wait()
+    g_wo.own()
+    spread1.stage0(1)
+    spread1.stage0(3)
+    spread1.stage0(2)
+    small_operands()
+    g_wgi.near()
+    g_wo.near()
+    spread1.stage1(3)
+    g_wgi.far()
+    spread1.stage1(1)
+    g_wgi.relay(2)
+    g_wo.far()
+    spread1.stage1(2)
+    g_wgi.relay(0)
+    spread1.stage1(0)
+    g_wgi.relay(1)
+    spread1.stage2(3)
+    g_wgi.relay(3)
+    g_wo.relay(3)
+    spread1.stage2(2)
+    g_wo.relay(2)
+    g_wo.relay(0)
+    g_wo.relay(1)
+    spread1.stage2(1)
+    local[4].wait()
+    local[5].wait()
+    g_wff.own()
+    spread1.stage2(0)
+    norm1(0)
+    g_wgi.done()
+    project(0)
+    scan(0)
+    g_wo.done()
+    mix_out(0)
+    norm1(1)
+    project(1)
+    sum1.stage1(0)
+    g_wff.near()
+    scan(1)
+    mix_out(1)
+    sum1.stage1(1)
+    sum1.stage2(0)
+    g_wff.relay(0)
+    g_wff.far()
+    local[6].wait()
+    g_wd.own()
+    norm1(2)
+    project(2)
+    sum1.stage2(1)
+    scan(2)
+    mix_out(2)
+    settle(0)
+    norm1(3)
+    project(3)
+    sum1.stage1(2)
+    settle(1)
+    g_wff.relay(2)
+    scan(3)
+    mix_out(3)
+    g_wff.relay(1)
+    sum1.stage2(2)
+    sum1.stage1(3)
+    g_wff.relay(3)
+    g_wd.near()
+    spread2.stage1(0)
+    spread2.stage1(1)
+    settle(2)
+    sum1.stage2(3)
+    spread2.stage2(0)
+    norm2(0)
+    spread2.stage2(1)
+    g_wff.done()
+    up(0)
+    spread2.stage1(2)
+    g_wd.far()
+    act(0)
+    norm2(1)
+    g_wd.relay(1)
+    up(1)
+    g_wd.relay(2)
+    settle(3)
+    spread2.stage2(2)
+    act(1)
+    g_wd.relay(0)
+    g_wd.relay(3)
+    norm2(2)
+    up(2)
+    act(2)
+    spread2.stage1(3)
+    g_wd.done()
+    down(0)
+    down(1)
+    down(2)
+    sum2.stage1(0)
+    sum2.stage1(1)
+    sum2.stage1(2)
+    spread2.stage2(3)
+    sum2.stage2(0)
+    norm2(3)
+    up(3)
+    sum2.stage2(2)
+    act(3)
+    down(3)
+    perm[...] = order((CH, CH), "sequence")
+    finish(0)
+    sum2.stage1(3)
+    sum2.stage2(1)
+    finish(2)
+    sum2.stage2(3)
+    finish(1)
+    finish(3)
 
     for gather in gathers:
         gather.drain()
 
-    def drained(c, carry):
+    for c in range(CHUNKS):
         for group in (spread1, spread2, sum1, sum2):
             group.drain(c)
-        return carry
-
-    lax.fori_loop(0, CHUNKS, drained, 0)
 
 
 def layer(*operands):

time: 124 us -> 108 us (0.87)
  Pallas kernels: 120 us -> 105 us
    pallas_call x1, Pallas kernels: 120 us -> 105 us  [layer(): pl.pallas_call(kernel, out_shape=jax.ShapeDtypeStruct((ROWS, CB), BF16),...]
where the time goes in v3:
time: 108 us
  Pallas kernels  105 us (97%)
  local copies, waits for them, and re-layouts  3.11 us (3%)
    pallas_call x1, Pallas kernels, layer(): pl.pallas_call(kernel, out_shape=jax.ShapeDtypeStruct((ROWS, CB), BF16),...  105 us
    unnamed x3, local copies, waits for them, and re-layouts  2.55 us

profile of v3, /device:TPU:1, one launch (start us, length us, event | category | flops | bytes accessed | tf_op | source)
XLA Modules:
  0.0 108.3 jit_solution(8263696100585078670)
XLA Ops:
  0.0 0.0 copy-start
  0.0 0.7 copy-done
  0.7 0.6 reshape.20.base_hbm
  1.2 105.1 %shard_map.136 = bf16[1024,256]{1,0:T(8,128)(2,1)} custom-call(bf16[352,128]{1,0:T(8,128)(2,1)} %bitcast.13, bf16[352,128]{1,0:T(8,128)(2,1)} %bitcast.14, bf16[1024,256]{1,0:T(8,128)(2,1)} %tok_hbm.1, bf16[352,128]{1,0:T(8,128)(2,1)} %wo_hbm.1, bf16[704,128]{1,0:T(8,128)(2,1)} %bitcast.11, bf16[704,128]{1,0:T(8,128)(2,1)} %bitcast.12, ...), custom_call_target="tpu_custom_call" | custom-call | tf_op jit(solution)/shard_map/pallas_call | solution.py:626
  106.4 1.9 %copy.16 = bf16[1024,256]{1,0:T(8,128)(2,1)} copy(bf16[1024,256]{1,0:T(8,128)(2,1)} %shard_map.136) | data formatting | bytes 1048576
Async XLA Ops:
  0.0 0.7 copy-start

commit v4 on v3

--- a/solution.py
+++ b/solution.py
@@ -395,7 +395,7 @@
         gm[0:R, RP : RP + R] = giv[...]
         small[...] = jnp.zeros_like(small)
         small[0:4, 0:R] = tapsv[...]
-        small[4:5, 0:R] = -GATE_EXPONENT * jax.nn.softplus(-basev[...])
+        small[4:5, 0:R] = -GATE_EXPONENT * jax.nn.softplus(-basev[...].reshape(1, R))
         for t in range(LEN):
             ldb[8 * t : 8 * t + 8, :] = jnp.broadcast_to(ldv[:, t : t + 1], (SEQS, 128))
         feat[0:24, :] = jnp.zeros((24, RP), F32)
@@ -558,9 +558,13 @@
     sum1.stage2(2)
     sum1.stage1(3)
     g_wff.relay(3)
+    for c in range(CHUNKS):
+        spread1.drain(c)
     g_wd.near()
     spread2.stage1(0)
     spread2.stage1(1)
+    g_wgi.drain()
+    g_wo.drain()
     settle(2)
     sum1.stage2(3)
     spread2.stage2(0)
@@ -592,6 +596,7 @@
     sum2.stage1(1)
     sum2.stage1(2)
     spread2.stage2(3)
+    g_wff.drain()
     sum2.stage2(0)
     norm2(3)
     up(3)
@@ -599,20 +604,21 @@
     act(3)
     down(3)
     perm[...] = order((CH, CH), "sequence")
+    g_wd.drain()
     finish(0)
     sum2.stage1(3)
     sum2.stage2(1)
+    for c in range(CHUNKS):
+        sum1.drain(c)
     finish(2)
+    for c in range(CHUNKS):
+        spread2.drain(c)
     sum2.stage2(3)
     finish(1)
     finish(3)
 
-    for gather in gathers:
-        gather.drain()
-
     for c in range(CHUNKS):
-        for group in (spread1, spread2, sum1, sum2):
-            group.drain(c)
+        sum2.drain(c)
 
 
 def layer(*operands):
@@ -641,7 +647,7 @@
             pltpu.VMEM((R, R), BF16),
             pltpu.VMEM((R, R), BF16),
             pltpu.VMEM((4, R), F32),
-            pltpu.VMEM((1, R), F32),
+            pltpu.VMEM((R,), F32),
             pltpu.VMEM((SEQS, LEN), F32),
             pltpu.VMEM((16, 128), F32),
             pltpu.VMEM((16, 128), F32),
@@ -699,7 +705,7 @@
         recurrence_gate_weight.reshape(R, R),
         input_gate_weight.reshape(R, R),
         convolution_taps,
-        base_decay_logit.reshape(1, R),
+        base_decay_logit,
         token_log_decay.reshape(SEQS, LEN),
         recurrence_norm_gain.reshape(16, 128),
         feedforward_norm_gain.reshape(16, 128),

time: 108 us -> 107 us (level)
  local copies, waits for them, and re-layouts: 3.11 us -> 1.87 us
    unnamed x3 -> x1, local copies, waits for them, and re-layouts: 2.55 us -> 1.87 us
where the time goes in v4:
time: 107 us
  Pallas kernels  105 us (98%)
  local copies, waits for them, and re-layouts  1.87 us (2%)
    pallas_call x1, Pallas kernels, layer(): pl.pallas_call(kernel, out_shape=jax.ShapeDtypeStruct((ROWS, CB), BF16),...  105 us

profile of v4, /device:TPU:1, one launch (start us, length us, event | category | flops | bytes accessed | tf_op | source)
XLA Modules:
  0.0 106.6 jit_solution(4610433778582369799)
XLA Ops:
  0.0 104.8 %shard_map.136 = bf16[1024,256]{1,0:T(8,128)(2,1)} custom-call(bf16[352,128]{1,0:T(8,128)(2,1)} %bitcast.13, bf16[352,128]{1,0:T(8,128)(2,1)} %bitcast.14, bf16[1024,256]{1,0:T(8,128)(2,1)} %tok_hbm.1, bf16[352,128]{1,0:T(8,128)(2,1)} %wo_hbm.1, bf16[704,128]{1,0:T(8,128)(2,1)} %bitcast.11, bf16[704,128]{1,0:T(8,128)(2,1)} %bitcast.12, ...), custom_call_target="tpu_custom_call" | custom-call | tf_op jit(solution)/shard_map/pallas_call | solution.py:632
  104.8 1.9 %copy.16 = bf16[1024,256]{1,0:T(8,128)(2,1)} copy(bf16[1024,256]{1,0:T(8,128)(2,1)} %shard_map.136) | data formatting | bytes 1048576

commit v5 on v4

--- a/solution.py
+++ b/solution.py
@@ -45,13 +45,30 @@
         span = pl.ds(lo[0], lo[1] + hi[1]) if half is None else pl.ds(*(lo, hi)[half])
         return self.buf.at[span, pl.ds(pl.multiple_of((z * SIDE + x) * 128, 128), 128)]
 
+    def group(self, k):
+        if k < 4:
+            return k // 2
+        return 6 if (k - 4) % 4 >= 2 else 2 + (k - 4) // 4
+
     def copy(self, view, part, k, to):
         return pltpu.make_async_remote_copy(
             src_ref=view,
             dst_ref=view,
-            send_sem=self.send.at[part, k],
-            recv_sem=self.recv.at[part, k],
+            send_sem=self.send,
+            recv_sem=self.recv.at[self.group(k)],
             device_id=to,
+            device_id_type=MESH,
+        )
+
+    def blocks(self, count, group):
+        (lo, hi), _ = self.rows
+        view = self.buf.at[pl.ds(0, 2 * (lo[1] + hi[1])), pl.ds(0, 128 * count)]
+        return pltpu.make_async_remote_copy(
+            src_ref=view,
+            dst_ref=view,
+            send_sem=self.send,
+            recv_sem=self.recv.at[group],
+            device_id=self.dev["x"][0],
             device_id_type=MESH,
         )
 
@@ -60,18 +77,6 @@
         (m1, i1, p1), (m2, i2, p2) = self.pos[a1], self.pos[a2]
         far1, far2 = lax.rem(i1 + 2, SIDE), lax.rem(i2 + 2, SIDE)
         return (i1, m1, p1, far1), (i2, m2, p2, far2), self.dev[a1], self.dev[a2]
-
-    def landing(self, part, k):
-        first, second, _, _ = self.places(part)
-        if k < 4:
-            where = (first[1], first[2], first[3], first[3])[k]
-            return self.block(part, where, second[0], None if k < 2 else k - 2)
-        q, k = divmod(k - 4, 4)
-        where = (second[1], second[2], second[3], second[3])[k]
-        return self.block(part, first[q], where, None if k < 2 else k - 2)
-
-    def arrived(self, part, k):
-        self.copy(self.landing(part, k), part, k, self.dev["x"][0]).wait_recv()
 
     def onto_second(self, part, q):
         first, second, _, dev2 = self.places(part)
@@ -89,40 +94,32 @@
             self.onto_second(part, 0)
 
     def near(self):
+        self.blocks(2, 0).wait_recv()
         for part in (0, 1):
             first, second, dev1, _ = self.places(part)
-            self.arrived(part, 0)
             self.copy(self.block(part, first[1], second[0], 0), part, 2, dev1[1]).start()
-            self.arrived(part, 1)
             self.copy(self.block(part, first[2], second[0], 1), part, 3, dev1[0]).start()
         for part in (0, 1):
             self.onto_second(part, 1)
             self.onto_second(part, 2)
 
     def far(self):
+        self.blocks(1, 1).wait_recv()
         for part in (0, 1):
-            self.arrived(part, 2)
-            self.arrived(part, 3)
             self.onto_second(part, 3)
 
     def relay(self, q):
+        self.blocks(2, 2 + q).wait_recv()
         for part in (0, 1):
             first, second, _, dev2 = self.places(part)
-            self.arrived(part, 4 + 4 * q)
             self.copy(self.block(part, first[q], second[1], 0), part, 6 + 4 * q, dev2[1]).start()
-            self.arrived(part, 5 + 4 * q)
             self.copy(self.block(part, first[q], second[2], 1), part, 7 + 4 * q, dev2[0]).start()
 
     def done(self):
-        for part in (0, 1):
-            for q in range(4):
-                self.arrived(part, 6 + 4 * q)
-                self.arrived(part, 7 + 4 * q)
+        self.blocks(4, 6).wait_recv()
 
     def drain(self):
-        for part in (0, 1):
-            for k in range(20):
-                self.copy(self.landing(part, k), part, k, self.dev["x"][0]).wait_send()
+        self.blocks(15, 0).wait_send()
 
 
 class Spread:
@@ -142,27 +139,22 @@
         return pltpu.make_async_remote_copy(
             src_ref=view,
             dst_ref=view,
-            send_sem=self.send.at[k, c],
-            recv_sem=self.recv.at[k, c],
+            send_sem=self.send,
+            recv_sem=self.recv.at[(0, 0, 2, 1, 1, 2, 2, 2)[k], c],
             device_id=to,
             device_id_type=MESH,
         )
 
-    def landing(self, k, c):
-        return [
-            (self.minus, None),
-            (self.plus, None),
-            (self.others[0], None),
-            (self.far, 0),
-            (self.far, 1),
-            (self.others[1], None),
-            (self.others[2], None),
-            (self.others[3], None),
-        ][k]
-
-    def arrived(self, k, c):
-        block, half = self.landing(k, c)
-        self.copy(self.view(block, c, half), k, c, self.dev["core"]).wait_recv()
+    def arrived(self, count, group, c):
+        view = self.buf.at[pl.ds(0, count), pl.ds(c * CH, CH), :]
+        pltpu.make_async_remote_copy(
+            src_ref=view,
+            dst_ref=view,
+            send_sem=self.send,
+            recv_sem=self.recv.at[group, c],
+            device_id=self.dev["core"],
+            device_id_type=MESH,
+        ).wait_recv()
 
     def stage0(self, c):
         view = self.view(self.own, c)
@@ -171,26 +163,29 @@
         self.copy(view, 2, c, self.dev["core"]).start()
 
     def stage1(self, c):
-        self.arrived(0, c)
+        self.arrived(2, 0, c)
         self.copy(self.view(self.minus, c, 0), 3, c, self.dev["y"][1]).start()
         self.copy(self.view(self.minus, c), 5, c, self.dev["core"]).start()
-        self.arrived(1, c)
         self.copy(self.view(self.plus, c, 1), 4, c, self.dev["y"][0]).start()
         self.copy(self.view(self.plus, c), 6, c, self.dev["core"]).start()
 
     def stage2(self, c):
-        self.arrived(3, c)
-        self.arrived(4, c)
+        self.arrived(1, 1, c)
         self.copy(self.view(self.far, c), 7, c, self.dev["core"]).start()
 
     def stage3(self, c):
-        for k in (2, 5, 6, 7):
-            self.arrived(k, c)
-
-    def drain(self, c):
-        for k in range(8):
-            block, half = self.landing(k, c)
-            self.copy(self.view(block, c, half), k, c, self.dev["core"]).wait_send()
+        self.arrived(4, 2, c)
+
+    def drain(self):
+        view = self.buf.at[pl.ds(0, 7)]
+        pltpu.make_async_remote_copy(
+            src_ref=view,
+            dst_ref=view,
+            send_sem=self.send,
+            recv_sem=self.recv.at[0, 0],
+            device_id=self.dev["core"],
+            device_id_type=MESH,
+        ).wait_send()
 
 
 class Sum:
@@ -220,11 +215,21 @@
         return pltpu.make_async_remote_copy(
             src_ref=src,
             dst_ref=dst,
-            send_sem=self.send.at[k, c],
-            recv_sem=self.recv.at[k, c],
+            send_sem=self.send,
+            recv_sem=self.recv.at[(k + 1) // 2, c],
             device_id=to,
             device_id_type=MESH,
         )
+
+    def arrived(self, view, group, c):
+        pltpu.make_async_remote_copy(
+            src_ref=view,
+            dst_ref=view,
+            send_sem=self.send,
+            recv_sem=self.recv.at[group, c],
+            device_id=self.dev["core"],
+            device_id_type=MESH,
+        ).wait_recv()
 
     def stage0(self, c):
         self.copy(0, c).start()
@@ -246,8 +251,8 @@
         add(self.own)
 
     def stage2(self, c):
+        self.arrived(self.halves.at[:, c], 1, c)
         for h, target in ((0, self.plus), (1, self.minus)):
-            self.copy(1 + h, c).wait_recv()
             rows = self.half(c, h)
             self.total[target, rows, :] = (
                 self.total[target, rows, :].astype(F32) + self.halves[h, c].astype(F32)
@@ -256,18 +261,24 @@
         self.copy(4, c).start()
 
     def stage3(self, c):
-        self.copy(3, c).wait_recv()
-        self.copy(4, c).wait_recv()
         rows = self.rows(c)
+        self.arrived(self.finals.at[:, rows, :], 2, c)
         return (
             self.total[self.own, rows, :].astype(F32)
             + self.finals[0, rows, :].astype(F32)
             + self.finals[1, rows, :].astype(F32)
         )
 
-    def drain(self, c):
-        for k in range(5):
-            self.copy(k, c).wait_send()
+    def drain(self, like):
+        view = like.at[pl.ds(0, 7)]
+        pltpu.make_async_remote_copy(
+            src_ref=view,
+            dst_ref=view,
+            send_sem=self.send,
+            recv_sem=self.recv.at[0, 0],
+            device_id=self.dev["core"],
+            device_id_type=MESH,
+        ).wait_send()
 
 
 def norm_chunk(full, gain, out, c):
@@ -558,8 +569,7 @@
     sum1.stage2(2)
     sum1.stage1(3)
     g_wff.relay(3)
-    for c in range(CHUNKS):
-        spread1.drain(c)
+    spread1.drain()
     g_wd.near()
     spread2.stage1(0)
     spread2.stage1(1)
@@ -608,17 +618,14 @@
     finish(0)
     sum2.stage1(3)
     sum2.stage2(1)
-    for c in range(CHUNKS):
-        sum1.drain(c)
+    sum1.drain(full1)
     finish(2)
-    for c in range(CHUNKS):
-        spread2.drain(c)
+    spread2.drain()
     sum2.stage2(3)
     finish(1)
     finish(3)
 
-    for c in range(CHUNKS):
-        sum2.drain(c)
+    sum2.drain(full2)
 
 
 def layer(*operands):
@@ -665,12 +672,12 @@
             pltpu.VMEM((ROWS, FFL), BF16),
             pltpu.VMEM((SEQS, RP), F32),
             pltpu.SemaphoreType.DMA((14,)),
-            pltpu.SemaphoreType.DMA((4, 2, 20)),
-            pltpu.SemaphoreType.DMA((4, 2, 20)),
-            pltpu.SemaphoreType.DMA((2, 8, CHUNKS)),
-            pltpu.SemaphoreType.DMA((2, 8, CHUNKS)),
-            pltpu.SemaphoreType.DMA((2, 5, CHUNKS)),
-            pltpu.SemaphoreType.DMA((2, 5, CHUNKS)),
+            pltpu.SemaphoreType.DMA((4,)),
+            pltpu.SemaphoreType.DMA((4, 7)),
+            pltpu.SemaphoreType.DMA((2,)),
+            pltpu.SemaphoreType.DMA((2, 3, CHUNKS)),
+            pltpu.SemaphoreType.DMA((2,)),
+            pltpu.SemaphoreType.DMA((2, 3, CHUNKS)),
         ],
         compiler_params=pltpu.CompilerParams(
             collective_id=0, has_side_effects=True, vmem_limit_bytes=66_000_000

time: 107 us -> 102 us (0.953)
  Pallas kernels: 105 us -> 100 us
    pallas_call x1, Pallas kernels: 105 us -> 100 us  [layer(): pl.pallas_call(kernel, out_shape=jax.ShapeDtypeStruct((ROWS, CB), BF16),...]
where the time goes in v5:
time: 102 us
  Pallas kernels  100 us (98%)
  local copies, waits for them, and re-layouts  1.87 us (2%)
    pallas_call x1, Pallas kernels, layer(): pl.pallas_call(kernel, out_shape=jax.ShapeDtypeStruct((ROWS, CB), BF16),...  100 us

profile of v5, /device:TPU:1, one launch (start us, length us, event | category | flops | bytes accessed | tf_op | source)
XLA Modules:
  0.0 102.0 jit_solution(15624335129256991200)
XLA Ops:
  0.0 100.2 %shard_map.136 = bf16[1024,256]{1,0:T(8,128)(2,1)} custom-call(bf16[352,128]{1,0:T(8,128)(2,1)} %bitcast.13, bf16[352,128]{1,0:T(8,128)(2,1)} %bitcast.14, bf16[1024,256]{1,0:T(8,128)(2,1)} %tok_hbm.1, bf16[352,128]{1,0:T(8,128)(2,1)} %wo_hbm.1, bf16[704,128]{1,0:T(8,128)(2,1)} %bitcast.11, bf16[704,128]{1,0:T(8,128)(2,1)} %bitcast.12, ...), custom_call_target="tpu_custom_call" | custom-call | tf_op jit(solution)/shard_map/pallas_call | solution.py:639
  100.2 1.9 %copy.16 = bf16[1024,256]{1,0:T(8,128)(2,1)} copy(bf16[1024,256]{1,0:T(8,128)(2,1)} %shard_map.136) | data formatting | bytes 1048576

commit v6 on v5

--- a/solution.py
+++ b/solution.py
@@ -300,7 +300,7 @@
                 out[here, lo : lo + 128] = (v[:, s * 128 : s * 128 + 128] * g).astype(BF16)
         return carry
 
-    lax.fori_loop(0, CH // step, body, 0, unroll=2)
+    lax.fori_loop(0, CH // step, body, 0, unroll=4)
 
 
 def order(shape, major):
@@ -455,7 +455,7 @@
             carried[rows, :] = (jnp.concatenate(states, axis=0) * jax.nn.gelu(proj[rows, :])).astype(BF16)
             return h
 
-        state[...] = lax.fori_loop(0, CH // 32, steps, state[...])
+        state[...] = lax.fori_loop(0, CH // 32, steps, state[...], unroll=2)
 
     def mix_out(c):
         rows = pl.ds(c * CH, CH)
@@ -503,38 +503,38 @@
         for s in range(SEQS):
             out[pl.ds(s * LEN + c * STEPS, STEPS), :] = ordered[s * STEPS : (s + 1) * STEPS]
 
-    g_wgi.own()
-    spread1.stage0(0)
     local[3].wait()
     g_wo.own()
+    spread1.stage0(0)
+    spread1.stage0(2)
+    g_wgi.own()
+    g_wo.near()
     spread1.stage0(1)
-    spread1.stage0(3)
-    spread1.stage0(2)
     small_operands()
     g_wgi.near()
-    g_wo.near()
+    spread1.stage1(1)
+    g_wo.far()
+    spread1.stage1(0)
+    spread1.stage0(3)
+    g_wgi.far()
+    g_wgi.relay(2)
+    g_wgi.relay(0)
+    spread1.stage1(2)
+    spread1.stage2(1)
+    g_wgi.relay(1)
+    g_wgi.relay(3)
+    g_wo.relay(1)
+    g_wo.relay(2)
+    g_wo.relay(3)
+    spread1.stage2(0)
+    g_wo.relay(0)
     spread1.stage1(3)
-    g_wgi.far()
-    spread1.stage1(1)
-    g_wgi.relay(2)
-    g_wo.far()
-    spread1.stage1(2)
-    g_wgi.relay(0)
-    spread1.stage1(0)
-    g_wgi.relay(1)
-    spread1.stage2(3)
-    g_wgi.relay(3)
-    g_wo.relay(3)
-    spread1.stage2(2)
-    g_wo.relay(2)
-    g_wo.relay(0)
-    g_wo.relay(1)
-    spread1.stage2(1)
+    local[6].wait()
+    g_wd.own()
+    norm1(0)
     local[4].wait()
     local[5].wait()
     g_wff.own()
-    spread1.stage2(0)
-    norm1(0)
     g_wgi.done()
     project(0)
     scan(0)
@@ -543,15 +543,13 @@
     norm1(1)
     project(1)
     sum1.stage1(0)
-    g_wff.near()
     scan(1)
     mix_out(1)
     sum1.stage1(1)
+    spread1.stage2(2)
     sum1.stage2(0)
-    g_wff.relay(0)
-    g_wff.far()
-    local[6].wait()
-    g_wd.own()
+    g_wff.near()
+    spread1.stage2(3)
     norm1(2)
     project(2)
     sum1.stage2(1)
@@ -559,41 +557,43 @@
     mix_out(2)
     settle(0)
     norm1(3)
+    sum1.stage1(2)
     project(3)
-    sum1.stage1(2)
+    scan(3)
+    g_wff.far()
     settle(1)
-    g_wff.relay(2)
-    scan(3)
-    mix_out(3)
+    spread2.stage1(0)
     g_wff.relay(1)
     sum1.stage2(2)
-    sum1.stage1(3)
+    g_wff.relay(2)
+    mix_out(3)
     g_wff.relay(3)
+    g_wff.relay(0)
     spread1.drain()
     g_wd.near()
-    spread2.stage1(0)
+    sum1.stage1(3)
     spread2.stage1(1)
     g_wgi.drain()
     g_wo.drain()
     settle(2)
-    sum1.stage2(3)
     spread2.stage2(0)
     norm2(0)
+    sum1.stage2(3)
     spread2.stage2(1)
     g_wff.done()
     up(0)
-    spread2.stage1(2)
     g_wd.far()
     act(0)
+    spread2.stage1(2)
+    g_wd.relay(0)
     norm2(1)
     g_wd.relay(1)
+    settle(3)
     up(1)
     g_wd.relay(2)
-    settle(3)
     spread2.stage2(2)
+    g_wd.relay(3)
     act(1)
-    g_wd.relay(0)
-    g_wd.relay(3)
     norm2(2)
     up(2)
     act(2)
@@ -601,28 +601,28 @@
     g_wd.done()
     down(0)
     down(1)
+    sum2.stage1(0)
     down(2)
-    sum2.stage1(0)
     sum2.stage1(1)
+    spread2.stage2(3)
     sum2.stage1(2)
-    spread2.stage2(3)
+    norm2(3)
     g_wff.drain()
     sum2.stage2(0)
-    norm2(3)
     up(3)
+    act(3)
+    sum2.stage2(1)
+    down(3)
+    sum2.stage1(3)
     sum2.stage2(2)
-    act(3)
-    down(3)
+    spread2.drain()
+    sum2.stage2(3)
+    sum1.drain(full1)
     perm[...] = order((CH, CH), "sequence")
+    finish(2)
+    finish(1)
     g_wd.drain()
     finish(0)
-    sum2.stage1(3)
-    sum2.stage2(1)
-    sum1.drain(full1)
-    finish(2)
-    spread2.drain()
-    sum2.stage2(3)
-    finish(1)
     finish(3)
 
     sum2.drain(full2)

time: 102 us -> 101 us (level)
  no operation moved by 1% of the time
where the time goes in v6:
time: 101 us
  Pallas kernels  99.4 us (98%)
  local copies, waits for them, and re-layouts  1.87 us (2%)
    pallas_call x1, Pallas kernels, layer(): pl.pallas_call(kernel, out_shape=jax.ShapeDtypeStruct((ROWS, CB), BF16),...  99.4 us

profile of v6, /device:TPU:1, one launch (start us, length us, event | category | flops | bytes accessed | tf_op | source)
XLA Modules:
  0.0 101.3 jit_solution(6838601270616320002)
XLA Ops:
  0.0 99.4 %shard_map.136 = bf16[1024,256]{1,0:T(8,128)(2,1)} custom-call(bf16[352,128]{1,0:T(8,128)(2,1)} %bitcast.13, bf16[352,128]{1,0:T(8,128)(2,1)} %bitcast.14, bf16[1024,256]{1,0:T(8,128)(2,1)} %tok_hbm.1, bf16[352,128]{1,0:T(8,128)(2,1)} %wo_hbm.1, bf16[704,128]{1,0:T(8,128)(2,1)} %bitcast.11, bf16[704,128]{1,0:T(8,128)(2,1)} %bitcast.12, ...), custom_call_target="tpu_custom_call" | custom-call | tf_op jit(solution)/shard_map/pallas_call | solution.py:639
  99.4 1.9 %copy.16 = bf16[1024,256]{1,0:T(8,128)(2,1)} copy(bf16[1024,256]{1,0:T(8,128)(2,1)} %shard_map.136) | data formatting | bytes 1048576

commit v7 on v6

--- a/solution.py
+++ b/solution.py
@@ -488,13 +488,20 @@
 
         lax.fori_loop(0, CH // 16, body, 0, unroll=2)
 
+    def products(rows, side):
+        for target in range(SIDE):
+            own_columns = pl.ds(pl.multiple_of((2 * target + side) * CB, CB), CB)
+            part2[target, side, rows, :] = jnp.dot(
+                hid[rows, :], wd[:, own_columns], preferred_element_type=F32
+            ).astype(BF16)
+
     def down(c):
         rows = pl.ds(c * CH, CH)
-        for j in range(8):
-            part2[j // 2, j % 2, rows, :] = jnp.dot(
-                hid[rows, :], wd[:, j * CB : (j + 1) * CB], preferred_element_type=F32
-            ).astype(BF16)
+        products(rows, 1 - core)
         sum2.stage0(c)
+
+    def keep(c):
+        products(pl.ds(c * CH, CH), core)
 
     def finish(c):
         rows = pl.ds(c * CH, CH)
@@ -505,38 +512,39 @@
 
     local[3].wait()
     g_wo.own()
+    spread1.stage0(3)
+    spread1.stage0(1)
     spread1.stage0(0)
     spread1.stage0(2)
     g_wgi.own()
     g_wo.near()
-    spread1.stage0(1)
     small_operands()
     g_wgi.near()
-    spread1.stage1(1)
+    g_wgi.far()
     g_wo.far()
     spread1.stage1(0)
-    spread1.stage0(3)
-    g_wgi.far()
+    g_wgi.relay(1)
     g_wgi.relay(2)
     g_wgi.relay(0)
+    spread1.stage1(1)
+    g_wgi.relay(3)
     spread1.stage1(2)
+    g_wo.relay(0)
+    g_wo.relay(3)
+    spread1.stage1(3)
     spread1.stage2(1)
-    g_wgi.relay(1)
-    g_wgi.relay(3)
+    g_wo.relay(2)
     g_wo.relay(1)
-    g_wo.relay(2)
-    g_wo.relay(3)
     spread1.stage2(0)
-    g_wo.relay(0)
-    spread1.stage1(3)
     local[6].wait()
     g_wd.own()
-    norm1(0)
     local[4].wait()
     local[5].wait()
     g_wff.own()
+    norm1(0)
     g_wgi.done()
     project(0)
+    spread1.stage2(2)
     scan(0)
     g_wo.done()
     mix_out(0)
@@ -545,49 +553,48 @@
     sum1.stage1(0)
     scan(1)
     mix_out(1)
-    sum1.stage1(1)
-    spread1.stage2(2)
-    sum1.stage2(0)
-    g_wff.near()
     spread1.stage2(3)
     norm1(2)
+    sum1.stage1(1)
+    g_wff.near()
+    sum1.stage2(0)
     project(2)
+    norm1(3)
+    scan(2)
     sum1.stage2(1)
-    scan(2)
+    g_wff.relay(0)
+    project(3)
     mix_out(2)
     settle(0)
-    norm1(3)
+    g_wff.far()
     sum1.stage1(2)
-    project(3)
-    scan(3)
-    g_wff.far()
     settle(1)
-    spread2.stage1(0)
-    g_wff.relay(1)
     sum1.stage2(2)
     g_wff.relay(2)
+    scan(3)
+    spread2.stage1(1)
+    g_wff.relay(1)
     mix_out(3)
+    spread2.stage1(0)
     g_wff.relay(3)
-    g_wff.relay(0)
-    spread1.drain()
-    g_wd.near()
     sum1.stage1(3)
-    spread2.stage1(1)
     g_wgi.drain()
     g_wo.drain()
     settle(2)
+    spread1.drain()
+    g_wd.near()
+    spread2.stage2(1)
     spread2.stage2(0)
     norm2(0)
     sum1.stage2(3)
-    spread2.stage2(1)
     g_wff.done()
     up(0)
+    spread2.stage1(2)
     g_wd.far()
+    g_wd.relay(0)
+    g_wd.relay(1)
     act(0)
-    spread2.stage1(2)
-    g_wd.relay(0)
     norm2(1)
-    g_wd.relay(1)
     settle(3)
     up(1)
     g_wd.relay(2)
@@ -601,28 +608,32 @@
     g_wd.done()
     down(0)
     down(1)
+    keep(0)
     sum2.stage1(0)
+    keep(1)
+    sum2.stage1(1)
     down(2)
-    sum2.stage1(1)
+    keep(2)
     spread2.stage2(3)
     sum2.stage1(2)
     norm2(3)
     g_wff.drain()
     sum2.stage2(0)
+    sum2.stage2(1)
     up(3)
     act(3)
-    sum2.stage2(1)
     down(3)
+    keep(3)
     sum2.stage1(3)
     sum2.stage2(2)
+    perm[...] = order((CH, CH), "sequence")
+    finish(1)
     spread2.drain()
     sum2.stage2(3)
-    sum1.drain(full1)
-    perm[...] = order((CH, CH), "sequence")
-    finish(2)
-    finish(1)
     g_wd.drain()
     finish(0)
+    sum1.drain(full1)
+    finish(2)
     finish(3)
 
     sum2.drain(full2)

time: 101 us -> 102 us (level)
  no operation moved by 1% of the time
where the time goes in v7:
time: 102 us
  Pallas kernels  99.6 us (98%)
  local copies, waits for them, and re-layouts  1.87 us (2%)
    pallas_call x1, Pallas kernels, layer(): pl.pallas_call(kernel, out_shape=jax.ShapeDtypeStruct((ROWS, CB), BF16),...  99.6 us

profile of v7, /device:TPU:1, one launch (start us, length us, event | category | flops | bytes accessed | tf_op | source)
XLA Modules:
  0.0 101.5 jit_solution(18282297879759113963)
XLA Ops:
  0.0 99.6 %shard_map.136 = bf16[1024,256]{1,0:T(8,128)(2,1)} custom-call(bf16[352,128]{1,0:T(8,128)(2,1)} %bitcast.13, bf16[352,128]{1,0:T(8,128)(2,1)} %bitcast.14, bf16[1024,256]{1,0:T(8,128)(2,1)} %tok_hbm.1, bf16[352,128]{1,0:T(8,128)(2,1)} %wo_hbm.1, bf16[704,128]{1,0:T(8,128)(2,1)} %bitcast.11, bf16[704,128]{1,0:T(8,128)(2,1)} %bitcast.12, ...), custom_call_target="tpu_custom_call" | custom-call | tf_op jit(solution)/shard_map/pallas_call | solution.py:650
  99.6 1.9 %copy.16 = bf16[1024,256]{1,0:T(8,128)(2,1)} copy(bf16[1024,256]{1,0:T(8,128)(2,1)} %shard_map.136) | data formatting | bytes 1048576
